TPU v7x, 32 devices: a whole 2x2x4 slice. The times are simulated.
32 devices in a mesh: sp: 4 (over z), fs: 4 (over y, core), tp: 2 (over x).
Axes of the slice: x: 2, y: 2, z: 4, core: 2. Of those that a mesh axis runs over, the one named last changes fastest.
Arguments:
- input_layer_rows: bfloat16 [4, 1024, 2048], P('fs', 'sp'), may hold values from -6 to 6
- input_norm_gain: float32 [2048], replicated, may hold values from 0.1 to 1.9
- query_weight_attention: bfloat16 [2048, 1024], P(('sp', 'fs'), 'tp'), may hold values from -0.125 to 0.125
- key_weight_attention: bfloat16 [2048, 1024], P(('sp', 'fs'), 'tp'), may hold values from -0.125 to 0.125
- value_weight_attention: bfloat16 [2048, 1024], P(('sp', 'fs'), 'tp'), may hold values from -0.125 to 0.125
- query_weight_recurrent: bfloat16 [2048, 1024], P(('sp', 'fs'), 'tp'), may hold values from -0.125 to 0.125
- forget_weight_recurrent: bfloat16 [2048, 1024], P(('sp', 'fs'), 'tp'), may hold values from -0.125 to 0.125
- value_weight_recurrent: bfloat16 [2048, 1024], P(('sp', 'fs'), 'tp'), may hold values from -0.125 to 0.125
- gate_weight_recurrent: bfloat16 [2048, 1024], P(('sp', 'fs'), 'tp'), may hold values from -0.125 to 0.125
- output_weight_attention: bfloat16 [2048, 1024], P(('sp', 'fs'), 'tp'), may hold values from -0.125 to 0.125
- emitted_projection_linear_scan: bfloat16 [2048, 1024], P(('sp', 'fs'), 'tp'), may hold values from -0.125 to 0.125
- score_offset: float32 [8], P('tp'), as said below
- attention_norm_gain: float32 [1024], P('tp'), may hold values from 0.1 to 1.9
- recurrence_norm_gain: float32 [1024], P('tp'), may hold values from 0.1 to 1.9
- forget_floor: float32 [1024], P('tp'), may hold values from 0.1 to 0.5
- forget_offset: float32 [1024], P('tp'), as said below
- extra_log_decay: float32 [4, 1024, 1024], P('fs', 'sp', 'tp')
Outputs:
- layer_out: bfloat16 [4, 1024, 2048], P('fs', ('sp', 'tp'))
- row_log_total: float32 [4, 8, 1024], P('fs', 'tp', 'sp')
Inputs may be any that keep to these rules, and one draw needn't show every extreme that they name: `score_offset`: each head's offset lies between -ln(1024) - 2 and -ln(1024) + 0.5. `forget_offset`: each channel's offset lies between ln(256) - 3 and ln(1024) + 0.6.
All inputs are finite; a program needn't handle non-finite values.
Results may differ from a plain program's by a relative error of at most 0.015.
Values may be sent and summed in bfloat16 or wider, within the bound.
A program may use at most 64 MiB of HBM per device.

v0:
```python
import functools
import jax
import jax.numpy as jnp
from jax import lax
from jax.experimental import pallas as pl
from jax.experimental.pallas import tpu as pltpu
from jax.sharding import PartitionSpec as P

HEAD = 128
BLOCK = 64


epsilon = 1e-06
log_floor = 0.05


def entering(shard, axis, combine, identity):
    size, index = (lax.axis_size(axis), lax.axis_index(axis))
    everything = jax.tree.map(
        lambda part, kind: lax.all_gather(part.astype(kind), axis),
        shard,
        (jnp.bfloat16, jnp.bfloat16),
    )
    start = jax.tree.map(
        lambda part, zero: jnp.broadcast_to(jnp.asarray(zero, part.dtype), part.shape),
        shard,
        identity,
    )

    def hop(k, before):
        reached = k < index
        new = combine(
            before, jax.tree.map(lambda part, own: part[k].astype(own.dtype), everything, shard)
        )
        return jax.tree.map(lambda a, b: jnp.where(reached, a, b), new, before)

    return lax.fori_loop(0, size, hop, start)


def head_norm(values, gain):
    square_mean = jnp.mean(values * values, axis=-1, keepdims=True)
    return values * lax.rsqrt(square_mean + epsilon) * gain


def recurrence_block(memory_matrix, inputs):
    query_slice, decay_part, key_slice, value_slice = inputs
    highest_score = lax.Precision.HIGHEST
    length = decay_part.shape[0]
    running_total = jnp.cumsum(decay_part, axis=0)
    causal = (
        lax.broadcasted_iota(jnp.int32, (length, length), 0)
        >= lax.broadcasted_iota(jnp.int32, (length, length), 1)
    )[:, :, None, None]
    relative = jnp.where(causal, running_total[:, None] - running_total[None, :], -jnp.inf)
    pairwise = jnp.sum(query_slice[:, None] * key_slice[None, :] * jnp.exp(relative), axis=-1)
    inner_part = jnp.einsum("tsh,shv->thv", pairwise, value_slice, precision=highest_score)
    carried_state = jnp.einsum(
        "fby,bym->fbm", query_slice * jnp.exp(running_total), memory_matrix, precision=highest_score
    )
    final_total = running_total[-1]
    updated_state = jnp.exp(final_total)[:, :, None] * memory_matrix + jnp.einsum(
        "rxc,rxa->xca",
        key_slice * jnp.exp(final_total[None] - running_total),
        value_slice,
        precision=highest_score,
    )
    return (updated_state, inner_part + carried_state)


def stick_piece(queries, shifts, weighted, keep_total, key_value, is_own, is_valid):
    scores = (
        jnp.einsum("thd,shd->hts", queries, key_value[0], preferred_element_type=jnp.float32)
        * HEAD ** (-0.5)
        + shifts[:, None, None]
    )
    logarithmic_retention = jax.nn.log_sigmoid(-scores)
    if is_own:
        rows_here = scores.shape[1]
        strict = lax.broadcasted_iota(jnp.int32, (rows_here, rows_here), 0) > lax.broadcasted_iota(
            jnp.int32, (rows_here, rows_here), 1
        )
        logarithmic_retention = jnp.where(strict, logarithmic_retention, 0.0)
    suffix = lax.cumsum(logarithmic_retention, axis=2, reverse=True) - logarithmic_retention
    log_weight = jax.nn.log_sigmoid(scores) + suffix + keep_total[:, :, None]
    if is_own:
        log_weight = jnp.where(strict, log_weight, -jnp.inf)
    weights = jnp.where(is_valid, jnp.exp(log_weight), 0.0).astype(jnp.bfloat16)
    weighted = weighted + jnp.einsum(
        "hts,shd->thd", weights, key_value[1], preferred_element_type=jnp.float32
    )
    keep_total = keep_total + jnp.where(is_valid, jnp.sum(logarithmic_retention, axis=2), 0.0)
    return (weighted, keep_total)


def contract_rows(rows_in, weight):
    return lax.dot_general(
        rows_in, weight, (((1,), (1,)), ((), ())), preferred_element_type=jnp.float32
    )


def on_device_general(
    input_layer_rows,
    input_norm_gain,
    query_weight_attention,
    key_weight_attention,
    value_weight_attention,
    query_weight_recurrent,
    forget_weight_recurrent,
    value_weight_recurrent,
    gate_weight_recurrent,
    output_weight_attention,
    emitted_projection_linear_scan,
    score_offset,
    attention_norm_gain,
    recurrence_norm_gain,
    forget_floor,
    forget_offset,
    extra_log_decay,
):
    values = input_layer_rows[0].astype(jnp.float32)
    square_mean = jnp.mean(values * values, axis=-1, keepdims=True)
    normed = (values * lax.rsqrt(square_mean + epsilon) * input_norm_gain).astype(jnp.bfloat16)
    tokens = normed.shape[0]
    weights_in = (
        query_weight_attention,
        key_weight_attention,
        value_weight_attention,
        query_weight_recurrent,
        forget_weight_recurrent,
        value_weight_recurrent,
        gate_weight_recurrent,
    )
    pieces = (
        lax.all_gather(weights_in[0], ("sp", "fs"), axis=0, tiled=True),
        lax.all_gather(weights_in[1], ("sp", "fs"), axis=0, tiled=True),
        lax.all_gather(weights_in[2], ("sp", "fs"), axis=0, tiled=True),
        lax.all_gather(weights_in[3], ("sp", "fs"), axis=0, tiled=True),
        lax.all_gather(weights_in[4], ("sp", "fs"), axis=0, tiled=True),
        lax.all_gather(weights_in[5], ("sp", "fs"), axis=0, tiled=True),
        lax.all_gather(weights_in[6], ("sp", "fs"), axis=0, tiled=True),
    )
    projected = tuple(
        (jnp.dot(normed, weight, preferred_element_type=jnp.float32) for weight in pieces)
    )
    query_a, key_a, value_a, query_b, forget_b, input_b, gate_b = [
        column_block.astype(jnp.bfloat16) for column_block in projected
    ]
    out_a, out_b = (
        lax.all_gather(output_weight_attention, ("sp", "fs"), axis=0, tiled=True),
        lax.all_gather(emitted_projection_linear_scan, ("sp", "fs"), axis=0, tiled=True),
    )
    head_count = query_a.shape[1] // HEAD
    queries = query_a.reshape(tokens, head_count, HEAD)
    key_value = jnp.stack(
        [key_a.reshape(tokens, head_count, HEAD), value_a.reshape(tokens, head_count, HEAD)]
    )
    weighted = jnp.zeros((tokens, head_count, HEAD), jnp.float32)
    keep_total = jnp.zeros((head_count, tokens), jnp.float32)
    weighted, keep_total = stick_piece(
        queries, score_offset, weighted, keep_total, key_value, True, True
    )
    position = lax.axis_index("sp")
    seq_devices = lax.axis_size("sp")
    gathered = lax.all_gather(key_value, "sp", axis=1, tiled=True)

    def gathered_turn(turn_index, carried_state):
        weighted_now, keep_now = carried_state
        source = jnp.maximum(position - turn_index, 0) * tokens
        piece_pair = lax.dynamic_slice_in_dim(gathered, source, tokens, 1)
        return stick_piece(
            queries, score_offset, weighted_now, keep_now, piece_pair, False, position >= turn_index
        )

    weighted, keep_total = lax.fori_loop(1, seq_devices, gathered_turn, (weighted, keep_total))
    row_log_total = jnp.log(jnp.maximum(-jnp.expm1(keep_total), log_floor))[None]
    mixed_a = (
        head_norm(weighted, attention_norm_gain.reshape(head_count, HEAD))
        .reshape(tokens, head_count * HEAD)
        .astype(jnp.bfloat16)
    )
    forget_logits = forget_b.astype(jnp.float32) + forget_offset
    forget_log_value = (
        jnp.logaddexp(
            jnp.log(forget_floor), jnp.log1p(-forget_floor) + jax.nn.log_sigmoid(forget_logits)
        )
        + extra_log_decay[0]
    )
    key_in = (1.0 - forget_floor) * jax.nn.sigmoid(-forget_logits)
    query_rows_input = jax.nn.silu(query_b.astype(jnp.float32)).reshape(tokens, head_count, HEAD)
    value_in = input_b.astype(jnp.float32)
    fading_channel_groups = forget_log_value.reshape(tokens, head_count, HEAD)
    shaped = tuple(
        (
            array_in.reshape(tokens // BLOCK, BLOCK, head_count, HEAD)
            for array_in in (query_rows_input, forget_log_value, key_in, value_in)
        )
    )
    empty_state = jnp.zeros((head_count, HEAD, HEAD), jnp.float32)
    nearby_hidden_vector, local_out = lax.scan(recurrence_block, empty_state, shaped)
    local_out = local_out.reshape(tokens, head_count, HEAD)
    through = jnp.exp(jnp.sum(fading_channel_groups, axis=0))

    def chain_states(earlier, later):
        return (earlier[0] * later[0], later[0][:, :, None] * earlier[1] + later[1])

    identity = (jnp.ones_like(through), jnp.zeros_like(nearby_hidden_vector))
    unused_decay, incoming_state = entering(
        (through, nearby_hidden_vector), "sp", chain_states, identity
    )
    running_sum = jnp.cumsum(fading_channel_groups, axis=0)
    recurrent = local_out + jnp.einsum(
        "fby,bym->fbm",
        query_rows_input * jnp.exp(running_sum),
        incoming_state,
        precision=lax.Precision.HIGHEST,
    )
    gated_out = head_norm(recurrent, recurrence_norm_gain.reshape(head_count, HEAD)) * jax.nn.silu(
        gate_b.astype(jnp.float32).reshape(tokens, head_count, HEAD)
    )
    mixed_b = gated_out.reshape(tokens, head_count * HEAD).astype(jnp.bfloat16)
    summed = lax.psum_scatter(
        (contract_rows(mixed_a, out_a) + contract_rows(mixed_b, out_b)).astype(jnp.bfloat16),
        "tp",
        scatter_dimension=0,
        tiled=True,
    )
    layer_out = summed[None]
    return (layer_out, row_log_total)


LEAF = 16
CHUNK = 128
TILE = 256
MESH = pl.DeviceIdType.MESH


def remote(src, dst, send, recv, **where):
    return pltpu.make_async_remote_copy(
        src_ref=src, dst_ref=dst, send_sem=send, recv_sem=recv, device_id=where, device_id_type=MESH
    )


def greet(peers):
    barrier = pltpu.get_barrier_semaphore()
    for where in peers:
        pl.semaphore_signal(barrier, inc=1, device_id=where, device_id_type=MESH)
    pl.semaphore_wait(barrier, len(peers))


def nt_dot(a, b):
    return lax.dot_general(a, b, (((1,), (1,)), ((), ())), preferred_element_type=jnp.float32)


def tn_dot(a, b):
    return lax.dot_general(a, b, (((0,), (0,)), ((), ())), preferred_element_type=jnp.float32)


def grid_of(shape):
    return lax.broadcasted_iota(jnp.int32, shape, 0), lax.broadcasted_iota(jnp.int32, shape, 1)


def attend_tile(i, p_ref, shift, gain):
    here = slice(i * TILE, (i + 1) * TILE)
    r, c = grid_of((TILE, TILE))
    later = (r > c).astype(jnp.bfloat16)
    query = p_ref[here, 0:HEAD]
    total = jnp.zeros((TILE, HEAD), jnp.float32)
    keep = jnp.zeros((TILE, 1), jnp.float32)
    for j in range(i, -1, -1):
        there = slice(j * TILE, (j + 1) * TILE)
        score = nt_dot(query, p_ref[there, HEAD : 2 * HEAD]) * HEAD ** (-0.5) + shift
        soft = -(jnp.maximum(score, 0.0) + jnp.log1p(jnp.exp(-jnp.abs(score))))
        held = jnp.where(r > c, soft, 0.0) if i == j else soft
        high = held.astype(jnp.bfloat16)
        low = (held - high.astype(jnp.float32)).astype(jnp.bfloat16)
        suffix = jnp.dot(high, later, preferred_element_type=jnp.float32) + jnp.dot(
            low, later, preferred_element_type=jnp.float32
        )
        weight = jnp.exp(score + soft + suffix + keep)
        if i == j:
            weight = jnp.where(r > c, weight, 0.0)
        total += jnp.dot(
            weight.astype(jnp.bfloat16),
            p_ref[there, 2 * HEAD : 3 * HEAD],
            preferred_element_type=jnp.float32,
        )
        keep += jnp.sum(held, axis=1, keepdims=True)
    return head_norm(total, gain).astype(jnp.bfloat16), keep


def recur_chunk(p_ref, e_ref, here, state, floor, offset, gain):
    r, c = grid_of((CHUNK, CHUNK))
    lower = (r >= c).astype(jnp.float32)
    part = lambda k: p_ref[here, k * HEAD : (k + 1) * HEAD].astype(jnp.float32)
    raw = part(3)
    query = raw * jax.nn.sigmoid(raw)
    key = (1.0 - floor) * jax.nn.sigmoid(-(part(4) + offset))
    value = p_ref[here, 5 * HEAD : 6 * HEAD]
    gate = part(6)
    decay = jnp.log1p(-key) + e_ref[...].astype(jnp.float32)
    run = jnp.dot(lower, decay, precision=lax.Precision.HIGHEST, preferred_element_type=jnp.float32)
    stripes = [jnp.zeros((LEAF, CHUNK), jnp.float32)]
    for s in range(LEAF, CHUNK, LEAF):
        edge = run[s - 1 : s, :]
        near = (query[s : s + LEAF] * jnp.exp(run[s : s + LEAF] - edge)).astype(jnp.bfloat16)
        far = (key * jnp.exp(jnp.where(r < s, edge - run, -jnp.inf))).astype(jnp.bfloat16)
        stripes.append(nt_dot(near, far))
    pairs = jnp.concatenate(stripes, axis=0)
    for d in range(LEAF):
        back_key = pltpu.roll(key, d, 0) if d else key
        back_run = pltpu.roll(run, d, 0) if d else run
        gap = jnp.where(r % LEAF >= d, run - back_run, -jnp.inf)
        column = jnp.sum(query * back_key * jnp.exp(gap), axis=1, keepdims=True)
        pairs = jnp.where((r - c == d) & (r % LEAF >= d), column, pairs)
    last = run[CHUNK - 1 : CHUNK, :]
    out = jnp.dot(pairs.astype(jnp.bfloat16), value, preferred_element_type=jnp.float32)
    out += nt_dot((query * jnp.exp(run)).astype(jnp.bfloat16), state.astype(jnp.bfloat16))
    mixed = head_norm(out, gain) * (gate * jax.nn.sigmoid(gate))
    state = jnp.exp(last) * state + tn_dot(value, (key * jnp.exp(last - run)).astype(jnp.bfloat16))
    return mixed.astype(jnp.bfloat16), state


PARTS = 4


def layer_kernel(n, *refs):
    raw_ref, g_ref, xe_ref, v_ref = refs[:4]
    w_refs, o_refs = refs[4:11], refs[11:13]
    out_ref, T = refs[13:15]
    (
        X, W, O, E, x_ref, e_ref, wp, proj, ma, mb, ts, M, away, landed,
        x_send, x_recv, xx_send, xx_recv,
        o_send, o_recv, oy_send, oy_recv, oc_send, oc_recv, od_send, od_recv,
        w_send, w_recv, wy_send, wy_recv, wc_send, wc_recv, wd_send, wd_recv,
        e_send, e_recv, m_send, m_recv, b_send, b_recv, t_send, t_recv, y_send, y_recv,
        pack_sem, local_sem,
    ) = refs[15:]
    z, f, x = lax.axis_index("sp"), lax.axis_index("fs"), lax.axis_index("tp")
    core, row, side = f + 1 - 2 * (f % 2), (f + 2) % 4, 1 - x
    tokens = x_ref.shape[0]
    half = tokens // 2
    step = half // PARTS
    both = (0, 1)

    def cols(h):
        return pl.ds(pl.multiple_of(h * HEAD, HEAD), HEAD)

    packs = []
    for i, w in enumerate(w_refs):
        for h in range(n):
            packs.append(
                pltpu.make_async_copy(
                    w.at[:, h * HEAD : (h + 1) * HEAD],
                    wp.at[h, :, i * HEAD : (i + 1) * HEAD],
                    pack_sem.at[i, h],
                )
            )
    wide = o_refs[0].shape[1]
    for i, o in enumerate(o_refs):
        packs.append(
            pltpu.make_async_copy(o, O.at[z, f, :, i * wide : (i + 1) * wide], local_sem.at[i])
        )
    for copy in packs:
        copy.start()
    barrier = pltpu.get_barrier_semaphore()
    peers = [{"sp": (z + o) % n} for o in range(1, n)] + [{"fs": core}, {"fs": row}, {"tp": side}]
    for where in peers:
        pl.semaphore_signal(barrier, inc=1, device_id=where, device_id_type=MESH)

    def normalise(i, carry):
        rows = pl.ds(pl.multiple_of(i * step, step), step)
        x_ref[rows, :] = head_norm(raw_ref[rows, :].astype(jnp.float32), g_ref[...]).astype(jnp.bfloat16)
        return carry

    lax.fori_loop(0, tokens // step, normalise, 0)
    for copy in packs:
        copy.wait()
    pl.semaphore_wait(barrier, len(peers))
    own_w = pltpu.make_async_copy(wp.at[z], W.at[z, f], local_sem.at[4])
    own_w.start()

    def reach(direction, k):
        if direction == 0:
            return (z - k >= 0) & (z + 1 < n), z - 1 - k >= 0, z - k, z - 1 - k, z + 1
        return (z + k < n) & (z - 1 >= 0), z + 1 + k < n, z + k, z + 1 + k, z - 1

    def span(c):
        return pl.ds(pl.multiple_of(x * half + c * step, step), step)

    def x_copy(direction, k, c, first=False):
        _, _, out, _, to = reach(direction, k)
        src = x_ref.at[span(c)] if first else X.at[out, span(c)]
        return remote(
            src, X.at[out, span(c)], x_send.at[direction, k, c], x_recv.at[direction, k, c], sp=to
        )

    def x_wait(direction, k, c):
        block = X.at[reach(direction, k)[3], span(c)]
        return remote(block, block, x_send.at[direction, k, c], x_recv.at[direction, k, c], sp=(z + 1) % n)

    def xx_copy(direction, k, c):
        block = X.at[reach(direction, k)[3], span(c)]
        return remote(block, block, xx_send.at[direction, k, c], xx_recv.at[direction, k, c], tp=side)

    def xx_wait(direction, k, c):
        there = pl.ds(pl.multiple_of(side * half + c * step, step), step)
        block = X.at[reach(direction, k)[3], there]
        return remote(block, block, xx_send.at[direction, k, c], xx_recv.at[direction, k, c], tp=side)

    def o_copy(direction, k):
        _, _, out, _, to = reach(direction, k)
        return remote(O.at[out, f], O.at[out, f], o_send.at[direction, k], o_recv.at[direction, k], sp=to)

    def o_side(kind, direction, k, own=False):
        block = z if own else reach(direction, k)[3]
        send, recv = ((oy_send, oy_recv), (oc_send, oc_recv), (od_send, od_recv))[kind]
        piece = O.at[block, row if kind == 2 else f]
        where = {"fs": row if kind == 0 else core}
        return remote(piece, piece, send.at[direction, k], recv.at[direction, k], **where)

    def o_own(kind):
        return o_side(kind, 2, 0, own=True)

    def w_copy(o):
        return remote(wp.at[(z + o) % n], W.at[z, f], w_send.at[o], w_recv.at[o], sp=(z + o) % n)

    def e_copy(o):
        return remote(e_ref.at[:, cols((z + o) % n)], E.at[z], e_send.at[o], e_recv.at[o], sp=(z + o) % n)

    def w_side(kind, o):
        block = (z - o + n) % n
        src = wp.at[z] if o == 0 else W.at[block, f]
        if kind == 0:
            return remote(src, W.at[block, f], wy_send.at[o], wy_recv.at[o], fs=row)
        if kind == 1:
            return remote(src, W.at[block, f], wc_send.at[o], wc_recv.at[o], fs=core)
        return remote(W.at[block, row], W.at[block, row], wd_send.at[o], wd_recv.at[o], fs=core)

    for d in both:
        @pl.when(reach(d, 0)[0])
        def _(d=d):
            for c in range(PARTS):
                x_copy(d, 0, c, True).start()
    for o in range(1, n):
        w_copy(o).start()
    for kind in both:
        w_side(kind, 0).start()
    local = [
        pltpu.make_async_copy(x_ref, X.at[z], local_sem.at[2]),
        pltpu.make_async_copy(e_ref.at[:, cols(z)], E.at[z], local_sem.at[3]),
    ]
    local[0].start()
    e_ref[...] = xe_ref[...].astype(jnp.bfloat16)

    def o_begin(direction, when):
        @pl.when(when & reach(direction, 0)[0])
        def _():
            o_copy(direction, 0).start()

    o_begin(0, z == 0)
    o_begin(1, z == n - 1)
    local[0].wait()
    own_w.wait()

    def project(block):
        rows = X[block]
        weights = W[...].reshape(rows.shape[1], W.shape[3])
        made = jnp.dot(rows, weights, preferred_element_type=jnp.float32)
        at = pl.ds(pl.multiple_of(block * tokens, tokens), tokens)
        proj[at, :] = made.astype(jnp.bfloat16)

    def gather_step(k, carry):
        for d in both:
            @pl.when((k < n - 1) & reach(d, k)[1])
            def _(d=d):
                for c in range(PARTS):
                    x_wait(d, k, c).wait_recv()

                    @pl.when(reach(d, k + 1)[0])
                    def _(c=c):
                        x_copy(d, k + 1, c).start()
                    xx_copy(d, k, c).start()

        @pl.when(k == max(n - 3, 0))
        def _():
            local[1].start()
            for o in range(1, n):
                e_copy(o).start()

        o_begin(0, (z > 0) & (k == z - 1))
        o_begin(1, (z < n - 1) & (k == n - 2 - z))

        @pl.when(k == 0)
        def _():
            for o in range(1, n):
                w_copy(o).wait_recv()
                for kind in both:
                    w_side(kind, o).start()
            for kind in both:
                o_own(kind).start()
            for o in range(n):
                w_side(0, o).wait_recv()
                w_side(2, o).start()
            for o in range(n):
                w_side(1, o).wait_recv()
                w_side(2, o).wait_recv()

        @pl.when(z - k >= 0)
        def _():
            @pl.when(k > 0)
            def _():
                for c in range(PARTS):
                    xx_wait(0, k - 1, c).wait_recv()
            project(z - k)

        @pl.when((k > 0) & (z + k < n))
        def _():
            for c in range(PARTS):
                xx_wait(1, k - 1, c).wait_recv()
            project(z + k)
        return carry

    lax.fori_loop(0, n, gather_step, 0)

    def o_tick(k):
        for d in both:
            @pl.when(reach(d, k)[1])
            def _(d=d):
                o_copy_in = O.at[reach(d, k)[3], f]
                remote(o_copy_in, o_copy_in, o_send.at[d, k], o_recv.at[d, k], sp=(z + 1) % n).wait_recv()
                if k + 1 < n - 1:
                    @pl.when(reach(d, k + 1)[0])
                    def _():
                        o_copy(d, k + 1).start()
                for kind in both:
                    o_side(kind, d, k).start()

    def m_copy(o):
        return remote(ma.at[(z + o) % n], M.at[0, z], m_send.at[o], m_recv.at[o], sp=(z + o) % n)

    def b_copy(o):
        return remote(mb.at[(z + o) % n], M.at[1, z], b_send.at[o], b_recv.at[o], sp=(z + o) % n)

    def t_copy(o):
        return remote(ts.at[(z + o) % n], T.at[z], t_send.at[o], t_recv.at[o], sp=(z + o) % n)

    o_tick(0)
    param = lambda i: v_ref[i, pl.ds(z, 1), :]
    shift = param(0)[:, 0:1]
    for i in range(n):
        mixed, keep = attend_tile(i, proj, shift, param(1))
        ma[i] = mixed
        total = jnp.log(jnp.maximum(1.0 - jnp.exp(keep), log_floor))
        ts[i] = jnp.broadcast_to(total, (tokens, HEAD)).T[0:8, :]
    local[1].wait()
    for o in range(1, n):
        e_copy(o).wait_recv()
    floor, offset, gain = param(3), param(4), param(2)
    per = tokens // CHUNK

    def chunk(i, state):
        here = pl.ds(pl.multiple_of(i * CHUNK, CHUNK), CHUNK)
        at = pl.ds(pl.multiple_of((i % per) * CHUNK, CHUNK), CHUNK)
        extra = E.at[i // per, at]
        mixed, state = recur_chunk(proj, extra, here, state, floor, offset, gain)
        mb[i // per, at, :] = mixed
        return state

    state = jnp.zeros((HEAD, HEAD), jnp.float32)
    count = per * n
    state = lax.fori_loop(0, count // 4, chunk, state)
    for o in range(1, n):
        m_copy(o).start()
    for o in range(1, n):
        t_copy(o).start()
    if n > 2:
        o_tick(1)
    lax.fori_loop(count // 4, count, chunk, state)
    mine = [
        pltpu.make_async_copy(ma.at[z], M.at[0, z], local_sem.at[5]),
        pltpu.make_async_copy(mb.at[z], M.at[1, z], local_sem.at[6]),
        pltpu.make_async_copy(ts.at[z], T.at[z], local_sem.at[7]),
    ]
    for copy in mine:
        copy.start()
    for o in range(1, n):
        b_copy(o).start()
    o_own(0).wait_recv()
    o_own(2).start()
    for k in range(2, n - 1):
        o_tick(k)
    o_own(1).wait_recv()
    o_own(2).wait_recv()
    for copy in mine:
        copy.wait()
    for o in range(1, n):
        m_copy(o).wait()
        b_copy(o).wait()

    shorter = jnp.minimum(z, n - 1 - z)

    def hop_of(s):
        t = s - 1
        paired = t < 2 * shorter
        k = jnp.where(paired, t // 2, t - shorter)
        d = jnp.where(paired, t % 2, jnp.where(z > n - 1 - z, 0, 1))
        return d, k, jnp.where(d == 0, z - 1 - k, z + 1 + k)

    def o_late(kind, s):
        d, k, block = hop_of(s)
        send, recv = ((oy_send, oy_recv), (oc_send, oc_recv), (od_send, od_recv))[kind]
        piece = O.at[block, row if kind == 2 else f]
        where = {"fs": row if kind == 0 else core}
        return remote(piece, piece, send.at[d, k], recv.at[d, k], **where)

    def rows_of(which):
        rows = pl.ds(pl.multiple_of(which * half, half), half)
        return jnp.concatenate([M[g, k, rows, :] for g in both for k in range(n)], axis=1)

    width = out_ref.shape[1] // n

    def y_copy(j):
        return remote(away.at[j], landed.at[j], y_send.at[j], y_recv.at[j], tp=side)

    def weights_of(block):
        return O[block].reshape(width, 2 * wide)

    theirs = rows_of(side)
    o_late(0, 1).wait_recv()
    o_late(2, 1).start()
    for j in range(n):
        if j:
            o_late(1, j).wait_recv()
            o_late(2, j).wait_recv()
        away[j] = nt_dot(theirs, weights_of(hop_of(j)[2] if j else z)).astype(jnp.bfloat16)
        if j:
            y_copy(j - 1).start()
            if j + 1 < n:
                o_late(0, j + 1).wait_recv()
                o_late(2, j + 1).start()
    ours = rows_of(x)
    for j in range(n):
        block = hop_of(j)[2] if j else z
        piece = nt_dot(ours, weights_of(block))
        if j == 0:
            y_copy(n - 1).start()
        y_copy(j).wait_recv()
        piece += landed[j].astype(jnp.float32)
        out_ref[:, pl.ds(pl.multiple_of(block * width, width), width)] = piece.astype(jnp.bfloat16)
    for j in range(n):
        y_copy(j).wait_send()
    for o in range(n):
        for kind in range(3):
            w_side(kind, o).wait_send()
    for o in range(1, n):
        t_copy(o).wait()
        e_copy(o).wait_send()
        w_copy(o).wait_send()
    for kind in range(3):
        o_own(kind).wait_send()
    for k in range(n - 1):
        for d in both:
            @pl.when(reach(d, k)[1])
            def _(d=d, k=k):
                for c in range(PARTS):
                    xx_copy(d, k, c).wait_send()
                for kind in range(3):
                    o_side(kind, d, k).wait_send()

            @pl.when(reach(d, k)[0])
            def _(d=d, k=k):
                for c in range(PARTS):
                    x_copy(d, k, c).wait_send()
                o_copy(d, k).wait_send()


VMEM = pl.BlockSpec(memory_space=pltpu.VMEM)
ANY = pl.BlockSpec(memory_space=pl.ANY)
DMA = pltpu.SemaphoreType.DMA


def on_device_heads(
    n,
    input_layer_rows,
    input_norm_gain,
    query_weight_attention,
    key_weight_attention,
    value_weight_attention,
    query_weight_recurrent,
    forget_weight_recurrent,
    value_weight_recurrent,
    gate_weight_recurrent,
    output_weight_attention,
    emitted_projection_linear_scan,
    score_offset,
    attention_norm_gain,
    recurrence_norm_gain,
    forget_floor,
    forget_offset,
    extra_log_decay,
):
    _, tokens, depth = input_layer_rows.shape
    groups = lax.axis_size("fs")
    share, columns = query_weight_attention.shape
    width = 7 * HEAD
    half = tokens // 2
    vectors = jnp.stack(
        [jnp.broadcast_to(score_offset[:, None], (n, HEAD))]
        + [
            v.reshape(n, HEAD)
            for v in (attention_norm_gain, recurrence_norm_gain, forget_floor, forget_offset)
        ]
    )
    bf = lambda *shape: pltpu.VMEM(shape, jnp.bfloat16)
    layer_out, T = pl.pallas_call(
        functools.partial(layer_kernel, n),
        out_shape=(
            jax.ShapeDtypeStruct((half, depth), jnp.bfloat16),
            jax.ShapeDtypeStruct((n, 8, tokens), jnp.float32),
        ),
        in_specs=[VMEM] * 4 + [ANY] * 9,
        out_specs=(VMEM,) * 2,
        scratch_shapes=[
            bf(n, tokens, depth),
            bf(n, groups, share, width),
            bf(n, groups, share, 2 * columns),
            bf(n, tokens, HEAD),
            bf(tokens, depth),
            bf(tokens, columns),
            bf(n, share, width),
            bf(n * tokens, width),
            bf(n, tokens, HEAD),
            bf(n, tokens, HEAD),
            pltpu.VMEM((n, 8, tokens), jnp.float32),
            bf(2, n, tokens, HEAD),
            bf(n, half, depth // n),
            bf(n, half, depth // n),
        ]
        + [DMA((2, n, PARTS))] * 4
        + [DMA((2, n))] * 2
        + [DMA((3, n))] * 6
        + [DMA((n,))] * 18
        + [DMA((7, n)), DMA((8,))],
        compiler_params=pltpu.CompilerParams(
            collective_id=0, has_side_effects=True, vmem_limit_bytes=56 * 1024 * 1024
        ),
    )(
        input_layer_rows[0],
        input_norm_gain[None],
        extra_log_decay[0],
        vectors,
        query_weight_attention,
        key_weight_attention,
        value_weight_attention,
        query_weight_recurrent,
        forget_weight_recurrent,
        value_weight_recurrent,
        gate_weight_recurrent,
        output_weight_attention,
        emitted_projection_linear_scan,
    )
    return (layer_out[None], T[:, 0, :][None])


def solution(mesh):
    n = mesh.shape["sp"]
    heads_fit = mesh.shape["fs"] == 4 and mesh.shape["tp"] == 2 and n > 1

    def on_device(*args):
        if heads_fit and args[11].shape[0] == n and args[0].shape[1] == TILE:
            return on_device_heads(n, *args)
        return on_device_general(*args)

    return jax.shard_map(
        on_device,
        mesh=mesh,
        in_specs=(
            P("fs", "sp", None),
            P(),
            P(("sp", "fs"), "tp"),
            P(("sp", "fs"), "tp"),
            P(("sp", "fs"), "tp"),
            P(("sp", "fs"), "tp"),
            P(("sp", "fs"), "tp"),
            P(("sp", "fs"), "tp"),
            P(("sp", "fs"), "tp"),
            P(("sp", "fs"), "tp"),
            P(("sp", "fs"), "tp"),
            P("tp"),
            P("tp"),
            P("tp"),
            P("tp"),
            P("tp"),
            P("fs", "sp", "tp"),
        ),
        out_specs=(P("fs", ("sp", "tp"), None), P("fs", "tp", "sp")),
        check_vma=False,
    )
```

profile of v0, /device:TPU:0, one launch (start us, length us, event | category | flops | bytes accessed | tf_op | source)
XLA Modules:
  0.0 122.8 jit_solution(1717661182295609130)
XLA Ops:
  0.6 0.0 copy-start.5
  0.6 0.0 copy-start.1
  0.6 0.6 copy-done.5
  1.3 0.1 constant_dynamic-update-slice_fusion.4
  1.4 0.0 copy-done.1
  1.4 0.0 copy-start.2
  1.4 0.7 copy-done.2
  2.0 0.0 copy-start.3
  2.1 0.7 copy-done.3
  2.7 0.0 copy-start.4
  2.7 0.7 copy-done.4
  3.4 0.0 copy-start
  3.4 0.6 copy-done
  4.0 115.5 %shard_map.176 = (bf16[128,2048]{1,0:T(8,128)(2,1)}, f32[4,8,256]{2,1,0:T(8,128)}) custom-call(bf16[256,2048]{1,0:T(8,128)(2,1)} %bitcast.14, f32[1,2048]{1,0:T(1,128)} %bitcast.17, f32[256,512]{1,0:T(8,128)} %bitcast.16, f32[5,4,128]{2,1,0:T(4,128)} %copy-done, bf16[128,512]{1,0:T(8,128)(2,1)} %refs_4_.1, bf16[128,512]{1,0:T(8,128)(2,1)} %refs_5_.1, ...), custom_call_target="tpu_custom_call" | custom-call | tf_op jit(solution)/shard_map/pallas_call | solution.py:715
  119.5 0.8 slice_bitcast_fusion
  120.3 0.6 copy.19
  120.9 1.9 %copy.25 = bf16[1,128,2048]{2,1,0:T(8,128)(2,1)} copy(bf16[1,128,2048]{2,1,0:T(8,128)(2,1)} %bitcast.15) | data formatting | bytes 1048576
  (4 shorter events, 0.0 us)
Async XLA Ops:
  0.6 0.7 copy-start.5
  0.6 0.7 copy-start.1
  1.4 0.7 copy-start.2
  2.0 0.7 copy-start.3
  2.7 0.7 copy-start.4
  3.4 0.6 copy-start
where the time goes:
time: 123 us
  Pallas kernels  116 us (94%)
  local copies, waits for them, and re-layouts  6.6 us (5%)
    pallas_call x1, Pallas kernels, on_device_heads(): pl.pallas_call(functools.partial(layer_kernel, n), out_shape=(jax.ShapeDt...  116 us
    unnamed x18, local copies, waits for them, and re-layouts  5.83 us

commit v1 on v0

--- a/solution.py
+++ b/solution.py
@@ -321,63 +321,70 @@
 
 
 PARTS = 4
+Y1A, Y1B, X1A, X1B, X2, Y2, C0, C1, C2, C3A, C3B = range(11)
+KINDS = 11
+OPEN = (Y1B, X1B, X1A, Y1A, C0)
+
+
+scope = jax.named_scope
 
 
 def layer_kernel(n, *refs):
-    raw_ref, g_ref, xe_ref, v_ref = refs[:4]
-    w_refs, o_refs = refs[4:11], refs[11:13]
-    out_ref, T = refs[13:15]
+    s_ref, g_ref, v_refs = refs[0], refs[1], refs[2:6]
+    raw_hbm, xe_hbm = refs[6:8]
+    w_refs, o_refs = refs[8:15], refs[15:17]
+    out_ref, T_ref = refs[17:19]
     (
-        X, W, O, E, x_ref, e_ref, wp, proj, ma, mb, ts, M, away, landed,
+        X, W, O, E, raw_ref, xe_ref, e_ref, wp, proj, ma, mb, ts, T, M, acc, done,
         x_send, x_recv, xx_send, xx_recv,
-        o_send, o_recv, oy_send, oy_recv, oc_send, oc_recv, od_send, od_recv,
+        oz_send, oz_recv, o_send, o_recv,
         w_send, w_recv, wy_send, wy_recv, wc_send, wc_recv, wd_send, wd_recv,
-        e_send, e_recv, m_send, m_recv, b_send, b_recv, t_send, t_recv, y_send, y_recv,
-        pack_sem, local_sem,
-    ) = refs[15:]
+        e_send, e_recv, m_send, m_recv, t_send, t_recv,
+        pack_sem, local_sem, out_sem,
+    ) = refs[19:]
     z, f, x = lax.axis_index("sp"), lax.axis_index("fs"), lax.axis_index("tp")
     core, row, side = f + 1 - 2 * (f % 2), (f + 2) % 4, 1 - x
-    tokens = x_ref.shape[0]
+    tokens = raw_ref.shape[0]
     half = tokens // 2
     step = half // PARTS
     both = (0, 1)
 
+    barrier = pltpu.get_barrier_semaphore()
+    peers = [{"sp": (z + o) % n} for o in range(1, n)] + [{"fs": core}, {"fs": row}, {"tp": side}]
+    peers += [{"sp": (z + o) % n, "tp": side} for o in range(1, n)]
+    for where in peers:
+        pl.semaphore_signal(barrier, inc=1, device_id=where, device_id_type=MESH)
+
     def cols(h):
         return pl.ds(pl.multiple_of(h * HEAD, HEAD), HEAD)
 
-    packs = []
-    for i, w in enumerate(w_refs):
-        for h in range(n):
-            packs.append(
-                pltpu.make_async_copy(
-                    w.at[:, h * HEAD : (h + 1) * HEAD],
-                    wp.at[h, :, i * HEAD : (i + 1) * HEAD],
-                    pack_sem.at[i, h],
-                )
+    def packs(o):
+        into = wp.at[o] if o else W.at[z, f]
+        return [
+            pltpu.make_async_copy(
+                w.at[:, cols((z + o) % n)], into.at[:, i * HEAD : (i + 1) * HEAD], pack_sem.at[i, o]
             )
-    wide = o_refs[0].shape[1]
-    for i, o in enumerate(o_refs):
-        packs.append(
-            pltpu.make_async_copy(o, O.at[z, f, :, i * wide : (i + 1) * wide], local_sem.at[i])
-        )
-    for copy in packs:
+            for i, w in enumerate(w_refs)
+        ]
+
+    def raw_half(which, sem):
+        rows = pl.ds(pl.multiple_of(which * half, half), half)
+        return pltpu.make_async_copy(raw_hbm.at[rows], raw_ref.at[rows], local_sem.at[sem])
+
+    loads = [
+        raw_half(x, 2),
+        raw_half(side, 5),
+        pltpu.make_async_copy(xe_hbm, xe_ref, local_sem.at[4]),
+    ] + [
+        pltpu.make_async_copy(o, O.at[z, f, x, i], local_sem.at[i])
+        for i, o in enumerate(o_refs)
+    ]
+    loads[0].start()
+    for copy in loads[3:]:
         copy.start()
-    barrier = pltpu.get_barrier_semaphore()
-    peers = [{"sp": (z + o) % n} for o in range(1, n)] + [{"fs": core}, {"fs": row}, {"tp": side}]
-    for where in peers:
-        pl.semaphore_signal(barrier, inc=1, device_id=where, device_id_type=MESH)
-
-    def normalise(i, carry):
-        rows = pl.ds(pl.multiple_of(i * step, step), step)
-        x_ref[rows, :] = head_norm(raw_ref[rows, :].astype(jnp.float32), g_ref[...]).astype(jnp.bfloat16)
-        return carry
-
-    lax.fori_loop(0, tokens // step, normalise, 0)
-    for copy in packs:
-        copy.wait()
-    pl.semaphore_wait(barrier, len(peers))
-    own_w = pltpu.make_async_copy(wp.at[z], W.at[z, f], local_sem.at[4])
-    own_w.start()
+    for o in range(n - 1, -1, -1):
+        for copy in packs(o):
+            copy.start()
 
     def reach(direction, k):
         if direction == 0:
@@ -387,12 +394,10 @@
     def span(c):
         return pl.ds(pl.multiple_of(x * half + c * step, step), step)
 
-    def x_copy(direction, k, c, first=False):
+    def x_copy(direction, k, c):
         _, _, out, _, to = reach(direction, k)
-        src = x_ref.at[span(c)] if first else X.at[out, span(c)]
-        return remote(
-            src, X.at[out, span(c)], x_send.at[direction, k, c], x_recv.at[direction, k, c], sp=to
-        )
+        block = X.at[out, span(c)]
+        return remote(block, block, x_send.at[direction, k, c], x_recv.at[direction, k, c], sp=to)
 
     def x_wait(direction, k, c):
         block = X.at[reach(direction, k)[3], span(c)]
@@ -407,60 +412,97 @@
         block = X.at[reach(direction, k)[3], there]
         return remote(block, block, xx_send.at[direction, k, c], xx_recv.at[direction, k, c], tp=side)
 
-    def o_copy(direction, k):
+    def o_copy(direction, k, m):
         _, _, out, _, to = reach(direction, k)
-        return remote(O.at[out, f], O.at[out, f], o_send.at[direction, k], o_recv.at[direction, k], sp=to)
-
-    def o_side(kind, direction, k, own=False):
-        block = z if own else reach(direction, k)[3]
-        send, recv = ((oy_send, oy_recv), (oc_send, oc_recv), (od_send, od_recv))[kind]
-        piece = O.at[block, row if kind == 2 else f]
-        where = {"fs": row if kind == 0 else core}
-        return remote(piece, piece, send.at[direction, k], recv.at[direction, k], **where)
-
-    def o_own(kind):
-        return o_side(kind, 2, 0, own=True)
+        piece = O.at[out, f, x, m]
+        return remote(piece, piece, oz_send.at[direction, k, m], oz_recv.at[direction, k, m], sp=to)
+
+    def o_side(kind, o):
+        block = (z - o + n) % n
+        y, across, chip = {"fs": row}, {"tp": side}, {"fs": core}
+        at, where = (
+            ((f, x, 0), y),
+            ((f, x, 1), y),
+            ((f, x, 0), across),
+            ((f, x, 1), across),
+            ((row, x, 1), across),
+            ((f, side, 0), y),
+            ((f, x), chip),
+            ((row, x), chip),
+            ((f, side), chip),
+            ((row, side, 0), chip),
+            ((row, side, 1), chip),
+        )[kind]
+        piece = O.at[(block, *at)]
+        return remote(piece, piece, o_send.at[kind, o], o_recv.at[kind, o], **where)
+
+    def slot(direction, k):
+        return k + 1 if direction == 0 else n - 1 - k
 
     def w_copy(o):
-        return remote(wp.at[(z + o) % n], W.at[z, f], w_send.at[o], w_recv.at[o], sp=(z + o) % n)
+        return remote(wp.at[o], W.at[z, f], w_send.at[o], w_recv.at[o], sp=(z + o) % n)
 
     def e_copy(o):
         return remote(e_ref.at[:, cols((z + o) % n)], E.at[z], e_send.at[o], e_recv.at[o], sp=(z + o) % n)
 
     def w_side(kind, o):
         block = (z - o + n) % n
-        src = wp.at[z] if o == 0 else W.at[block, f]
-        if kind == 0:
-            return remote(src, W.at[block, f], wy_send.at[o], wy_recv.at[o], fs=row)
-        if kind == 1:
-            return remote(src, W.at[block, f], wc_send.at[o], wc_recv.at[o], fs=core)
-        return remote(W.at[block, row], W.at[block, row], wd_send.at[o], wd_recv.at[o], fs=core)
-
+        piece = W.at[block, row if kind == 2 else f]
+        send, recv = ((wy_send, wy_recv), (wc_send, wc_recv), (wd_send, wd_recv))[kind]
+        where = {"fs": row if kind == 0 else core}
+        return remote(piece, piece, send.at[o], recv.at[o], **where)
+
+    for copy in loads[1:3]:
+        copy.start()
+
+    def normalise(i, which):
+        rows = pl.ds(pl.multiple_of(which * half + i * step, step), step)
+        X[z, rows, :] = head_norm(raw_ref[rows, :].astype(jnp.float32), g_ref[...]).astype(jnp.bfloat16)
+        return which
+
+    def o_begin(when):
+        for d in both:
+            @pl.when(when(z if d == 0 else n - 1 - z))
+            def _(d=d):
+                for m in (1, 0):
+                    o_copy(d, 0, m).start()
+
+    loads[0].wait()
+    with scope("norm"):
+        lax.fori_loop(0, PARTS, normalise, x)
+    with scope("packs"):
+        for o in range(n):
+            for copy in packs(o):
+                copy.wait()
+    for copy in loads[3:]:
+        copy.wait()
+    with scope("barrier"):
+        pl.semaphore_wait(barrier, len(peers))
+    o_begin(lambda at: (at == 0) | (at == n - 2))
     for d in both:
         @pl.when(reach(d, 0)[0])
         def _(d=d):
             for c in range(PARTS):
-                x_copy(d, 0, c, True).start()
-    for o in range(1, n):
-        w_copy(o).start()
+                x_copy(d, 0, c).start()
+    for far in range(n - 1, 0, -1):
+        @pl.when(z + far < n)
+        def _(far=far):
+            w_copy(far).start()
+
+        @pl.when(z - far >= 0)
+        def _(far=far):
+            w_copy(n - far).start()
     for kind in both:
         w_side(kind, 0).start()
-    local = [
-        pltpu.make_async_copy(x_ref, X.at[z], local_sem.at[2]),
-        pltpu.make_async_copy(e_ref.at[:, cols(z)], E.at[z], local_sem.at[3]),
-    ]
-    local[0].start()
+    for copy in loads[1:3]:
+        copy.wait()
+    o_begin(lambda at: (at > 0) & (at < n - 2))
+    for kind in OPEN:
+        o_side(kind, 0).start()
+    lax.fori_loop(0, PARTS, normalise, side)
     e_ref[...] = xe_ref[...].astype(jnp.bfloat16)
-
-    def o_begin(direction, when):
-        @pl.when(when & reach(direction, 0)[0])
-        def _():
-            o_copy(direction, 0).start()
-
-    o_begin(0, z == 0)
-    o_begin(1, z == n - 1)
-    local[0].wait()
-    own_w.wait()
+    local = [None, pltpu.make_async_copy(e_ref.at[:, cols(z)], E.at[z], local_sem.at[3])]
+    local[1].start()
 
     def project(block):
         rows = X[block]
@@ -469,94 +511,242 @@
         at = pl.ds(pl.multiple_of(block * tokens, tokens), tokens)
         proj[at, :] = made.astype(jnp.bfloat16)
 
+    def x_relay(d, k, c):
+        x_wait(d, k, c).wait_recv()
+
+        @pl.when(reach(d, k + 1)[0])
+        def _():
+            x_copy(d, k + 1, c).start()
+        xx_copy(d, k, c).start()
+
+    def w_arrived(o):
+        with scope("wz"):
+            w_copy(o).wait_recv()
+        for kind in both:
+            w_side(kind, o).start()
+
+    def w_crossed(o):
+        with scope("wy"):
+            w_side(0, o).wait_recv()
+        w_side(2, o).start()
+
+    def o_pass(o, *pairs):
+        for got, then in pairs:
+            o_side(got, o).wait_recv()
+            o_side(then, o).start()
+
+    def o_seen_x(o):
+        o_pass(o, (X1A, Y2), (X1B, C2))
+
+    def o_seen_y(o):
+        o_pass(o, (Y1B, X2), (Y1A, C1))
+
+    def o_seen(o):
+        o_seen_x(o)
+        o_seen_y(o)
+
+    def o_across(o):
+        o_pass(o, (X2, C3B), (Y2, C3A))
+
+    def o_relay(d, k, halves=(1, 0)):
+        if k + 1 < n - 1:
+            @pl.when(reach(d, k + 1)[0])
+            def _():
+                for m in halves:
+                    o_copy(d, k + 1, m).start()
+
+    def o_half(d, k, m, kinds, relay=True):
+        piece = O.at[reach(d, k)[3], f, x, m]
+        remote(piece, piece, oz_send.at[d, k, m], oz_recv.at[d, k, m], sp=(z + 1) % n).wait_recv()
+        if relay:
+            o_relay(d, k, (m,))
+        for kind in kinds:
+            o_side(kind, slot(d, k)).start()
+
+    def o_first(d, k, relay=True):
+        o_half(d, k, 1, (Y1B, X1B), relay)
+
+    def o_second(d, k, relay=True):
+        o_half(d, k, 0, (X1A, Y1A, C0), relay)
+
+    def o_full(d, k):
+        o_first(d, k)
+        o_second(d, k)
+
+    def o_near(d, k):
+        o_first(d, k, False)
+        o_second(d, k, False)
+
+    def each(k, when, do):
+        for d in both:
+            at = z if d == 0 else n - 1 - z
+            @pl.when((at - 1 - k >= 0) & when(at))
+            def _(d=d):
+                do(d, k)
+
+    look = lambda d, k: o_seen(slot(d, k))
+    over = lambda d, k: o_across(slot(d, k))
+    early = lambda at: (at == 1) | (at == n - 1)
+    late = lambda at: (at != 1) & (at != n - 1)
+    last = lambda at: at == n - 1
+    inner = lambda at: at != n - 1
+    always = lambda at: at >= 0
+
+    def w_each(do, far, when):
+        for d in both:
+            at = z if d == 0 else n - 1 - z
+            @pl.when((at - far >= 0) & when(at))
+            def _(o=far if d == 0 else n - far):
+                do(o)
+
+    def x_hop(k, c):
+        for d in both:
+            @pl.when(reach(d, k)[1])
+            def _(d=d):
+                with scope("xk%d" % k):
+                    x_relay(d, k, c)
+
+    with scope("oearly"):
+        each(0, early, o_near)
+    x_hop(0, 0)
+    with scope("own"):
+        o_seen(0)
+    x_hop(0, 1)
+    with scope("seenx"):
+        each(0, early, lambda d, k: o_seen_x(slot(d, k)))
+    x_hop(0, 2)
+    with scope("seeny"):
+        each(0, early, lambda d, k: o_seen_y(slot(d, k)))
+    x_hop(0, 3)
+    each(0, lambda at: at == 1, o_relay)
+    w_crossed(0)
+    w_each(w_arrived, 1, lambda at: at != 2)
+    for far in range(2, n):
+        w_each(w_arrived, far, always)
+    w_each(w_arrived, 1, lambda at: at == 2)
+    with scope("across0"):
+        o_across(0)
+        each(0, early, over)
+    with scope("omid"):
+        each(0, lambda at: at == 2, o_full)
+    for c in range(PARTS):
+        x_hop(1, c)
+    w_each(w_crossed, 1, lambda at: at != 2)
+    for far in range(2, n):
+        w_each(w_crossed, far, always)
+    w_each(w_crossed, 1, lambda at: at == 2)
+    with scope("o31"):
+        each(1, lambda at: at > 2, o_first)
+        each(1, lambda at: at > 2, lambda d, k: o_half(d, k, 0, (Y1A, C0)))
+
+    def e_begin():
+        for o in range(1, n):
+            e_copy(o).start()
+
+    outer = (z == 0) | (z == n - 1)
+    with scope("wc"):
+        for o in range(n):
+            w_side(1, o).wait_recv()
+            w_side(2, o).wait_recv()
+
     def gather_step(k, carry):
-        for d in both:
-            @pl.when((k < n - 1) & reach(d, k)[1])
-            def _(d=d):
-                for c in range(PARTS):
-                    x_wait(d, k, c).wait_recv()
-
-                    @pl.when(reach(d, k + 1)[0])
-                    def _(c=c):
-                        x_copy(d, k + 1, c).start()
-                    xx_copy(d, k, c).start()
-
-        @pl.when(k == max(n - 3, 0))
+        @pl.when(k == 1)
         def _():
-            local[1].start()
-            for o in range(1, n):
-                e_copy(o).start()
-
-        o_begin(0, (z > 0) & (k == z - 1))
-        o_begin(1, (z < n - 1) & (k == n - 2 - z))
-
-        @pl.when(k == 0)
+            with scope("seeny"):
+                each(0, lambda at: at == 2, look)
+
+        @pl.when(k == n - 1)
         def _():
-            for o in range(1, n):
-                w_copy(o).wait_recv()
-                for kind in both:
-                    w_side(kind, o).start()
-            for kind in both:
-                o_own(kind).start()
-            for o in range(n):
-                w_side(0, o).wait_recv()
-                w_side(2, o).start()
-            for o in range(n):
-                w_side(1, o).wait_recv()
-                w_side(2, o).wait_recv()
+            with scope("o21"):
+                each(1, lambda at: at == 2, o_full)
+            each(1, lambda at: at > 2, lambda d, k: o_side(X1A, slot(d, k)).start())
+            with scope("look31"):
+                each(1, lambda at: at > 2, lambda d, k: o_seen_y(slot(d, k)))
+
+        pl.when((k == 2) & outer)(e_begin)
+        pl.when((k == 3) & jnp.logical_not(outer))(e_begin)
 
         @pl.when(z - k >= 0)
         def _():
             @pl.when(k > 0)
             def _():
                 for c in range(PARTS):
-                    xx_wait(0, k - 1, c).wait_recv()
-            project(z - k)
+                    with scope("xx"):
+                        xx_wait(0, k - 1, c).wait_recv()
+            with scope("proj"):
+                project(z - k)
 
         @pl.when((k > 0) & (z + k < n))
         def _():
             for c in range(PARTS):
-                xx_wait(1, k - 1, c).wait_recv()
-            project(z + k)
+                with scope("xx"):
+                    xx_wait(1, k - 1, c).wait_recv()
+            with scope("proj"):
+                project(z + k)
+
+        @pl.when(k < n - 1)
+        def _():
+            x_hop(2, k + 1)
         return carry
 
+    x_hop(2, 0)
     lax.fori_loop(0, n, gather_step, 0)
-
-    def o_tick(k):
-        for d in both:
-            @pl.when(reach(d, k)[1])
-            def _(d=d):
-                o_copy_in = O.at[reach(d, k)[3], f]
-                remote(o_copy_in, o_copy_in, o_send.at[d, k], o_recv.at[d, k], sp=(z + 1) % n).wait_recv()
-                if k + 1 < n - 1:
-                    @pl.when(reach(d, k + 1)[0])
-                    def _():
-                        o_copy(d, k + 1).start()
-                for kind in both:
-                    o_side(kind, d, k).start()
-
-    def m_copy(o):
-        return remote(ma.at[(z + o) % n], M.at[0, z], m_send.at[o], m_recv.at[o], sp=(z + o) % n)
-
-    def b_copy(o):
-        return remote(mb.at[(z + o) % n], M.at[1, z], b_send.at[o], b_recv.at[o], sp=(z + o) % n)
+    with scope("over0"):
+        each(0, lambda at: at == 2, over)
+
+    def m_copy(m, flip, o):
+        to = side if flip else x
+        rows = pl.ds(pl.multiple_of(to * half, half), half)
+        src = (ma, mb)[m].at[(z + o) % n, rows]
+        sems = m_send.at[m, flip, o], m_recv.at[m, flip, o]
+        if o == 0 and not flip:
+            return pltpu.make_async_copy(src, M.at[m, x, z], sems[1])
+        return remote(src, M.at[m, x, z], *sems, sp=(z + o) % n, tp=to)
 
     def t_copy(o):
+        if o == 0:
+            return pltpu.make_async_copy(ts.at[z], T.at[z], t_recv.at[o])
         return remote(ts.at[(z + o) % n], T.at[z], t_send.at[o], t_recv.at[o], sp=(z + o) % n)
 
-    o_tick(0)
-    param = lambda i: v_ref[i, pl.ds(z, 1), :]
-    shift = param(0)[:, 0:1]
+    ways = [(flip, o) for o in range(n - 1, -1, -1) for flip in both]
+
+    param = lambda i: v_refs[i][:, cols(z)]
+    shift = s_ref[z]
     for i in range(n):
-        mixed, keep = attend_tile(i, proj, shift, param(1))
+        with scope('attn'):
+            mixed, keep = attend_tile(i, proj, shift, param(0))
         ma[i] = mixed
         total = jnp.log(jnp.maximum(1.0 - jnp.exp(keep), log_floor))
         ts[i] = jnp.broadcast_to(total, (tokens, HEAD)).T[0:8, :]
+    with scope("o32"):
+        each(2, always, o_first)
     local[1].wait()
-    for o in range(1, n):
-        e_copy(o).wait_recv()
-    floor, offset, gain = param(3), param(4), param(2)
+    with scope('ewait'):
+        for o in range(1, n):
+            e_copy(o).wait_recv()
+    floor, offset, gain = param(2), param(3), param(1)
     per = tokens // CHUNK
+
+    def tick0():
+        each(2, always, o_second)
+        each(1, lambda at: at > 2, lambda d, k: o_seen_x(slot(d, k)))
+
+    def tick1():
+        each(1, lambda at: at == 2, look)
+
+    def tick3():
+        for way in ways:
+            m_copy(0, *way).start()
+        for o in range(n):
+            t_copy(o).start()
+
+    def tick5():
+        each(1, lambda at: at > 2, over)
+        each(1, lambda at: at == 2, over)
+        each(2, always, lambda d, k: o_seen_x(slot(d, k)))
+
+    count = per * n
+    ticks = ((0, tick0), (1, tick1), (3, tick3), (5, tick5))
 
     def chunk(i, state):
         here = pl.ds(pl.multiple_of(i * CHUNK, CHUNK), CHUNK)
@@ -564,117 +754,128 @@
         extra = E.at[i // per, at]
         mixed, state = recur_chunk(proj, extra, here, state, floor, offset, gain)
         mb[i // per, at, :] = mixed
+        for when, tick in ticks:
+            @pl.when(i == when)
+            def _(when=when, tick=tick):
+                with scope("tick%d" % when):
+                    tick()
         return state
 
     state = jnp.zeros((HEAD, HEAD), jnp.float32)
-    count = per * n
-    state = lax.fori_loop(0, count // 4, chunk, state)
-    for o in range(1, n):
-        m_copy(o).start()
-    for o in range(1, n):
-        t_copy(o).start()
-    if n > 2:
-        o_tick(1)
-    lax.fori_loop(count // 4, count, chunk, state)
-    mine = [
-        pltpu.make_async_copy(ma.at[z], M.at[0, z], local_sem.at[5]),
-        pltpu.make_async_copy(mb.at[z], M.at[1, z], local_sem.at[6]),
-        pltpu.make_async_copy(ts.at[z], T.at[z], local_sem.at[7]),
-    ]
-    for copy in mine:
-        copy.start()
-    for o in range(1, n):
-        b_copy(o).start()
-    o_own(0).wait_recv()
-    o_own(2).start()
-    for k in range(2, n - 1):
-        o_tick(k)
-    o_own(1).wait_recv()
-    o_own(2).wait_recv()
-    for copy in mine:
-        copy.wait()
-    for o in range(1, n):
-        m_copy(o).wait()
-        b_copy(o).wait()
-
-    shorter = jnp.minimum(z, n - 1 - z)
-
-    def hop_of(s):
+    with scope("rec"):
+        lax.fori_loop(0, count, chunk, state)
+    for way in ways:
+        m_copy(1, *way).start()
+    with scope("end2"):
+        each(2, always, lambda d, k: o_seen_y(slot(d, k)))
+    with scope("end3"):
+        each(2, always, over)
+
+    with scope("drain"):
+        for o in range(n):
+            for kind in range(3):
+                w_side(kind, o).wait_send()
+        for o in range(1, n):
+            e_copy(o).wait_send()
+            w_copy(o).wait_send()
+        for k in range(n - 1):
+            for d in both:
+                @pl.when(reach(d, k)[1])
+                def _(d=d, k=k):
+                    for c in range(PARTS):
+                        xx_copy(d, k, c).wait_send()
+
+                @pl.when(reach(d, k)[0])
+                def _(d=d, k=k):
+                    for c in range(PARTS):
+                        x_copy(d, k, c).wait_send()
+                    for m in both:
+                        o_copy(d, k, m).wait_send()
+
+    def order(s):
+        shorter = jnp.minimum(z, n - 1 - z)
         t = s - 1
         paired = t < 2 * shorter
         k = jnp.where(paired, t // 2, t - shorter)
         d = jnp.where(paired, t % 2, jnp.where(z > n - 1 - z, 0, 1))
-        return d, k, jnp.where(d == 0, z - 1 - k, z + 1 + k)
-
-    def o_late(kind, s):
-        d, k, block = hop_of(s)
-        send, recv = ((oy_send, oy_recv), (oc_send, oc_recv), (od_send, od_recv))[kind]
-        piece = O.at[block, row if kind == 2 else f]
-        where = {"fs": row if kind == 0 else core}
-        return remote(piece, piece, send.at[d, k], recv.at[d, k], **where)
-
-    def rows_of(which):
-        rows = pl.ds(pl.multiple_of(which * half, half), half)
-        return jnp.concatenate([M[g, k, rows, :] for g in both for k in range(n)], axis=1)
-
-    width = out_ref.shape[1] // n
-
-    def y_copy(j):
-        return remote(away.at[j], landed.at[j], y_send.at[j], y_recv.at[j], tp=side)
-
-    def weights_of(block):
-        return O[block].reshape(width, 2 * wide)
-
-    theirs = rows_of(side)
-    o_late(0, 1).wait_recv()
-    o_late(2, 1).start()
-    for j in range(n):
-        if j:
-            o_late(1, j).wait_recv()
-            o_late(2, j).wait_recv()
-        away[j] = nt_dot(theirs, weights_of(hop_of(j)[2] if j else z)).astype(jnp.bfloat16)
-        if j:
-            y_copy(j - 1).start()
-            if j + 1 < n:
-                o_late(0, j + 1).wait_recv()
-                o_late(2, j + 1).start()
-    ours = rows_of(x)
-    for j in range(n):
-        block = hop_of(j)[2] if j else z
-        piece = nt_dot(ours, weights_of(block))
-        if j == 0:
-            y_copy(n - 1).start()
-        y_copy(j).wait_recv()
-        piece += landed[j].astype(jnp.float32)
-        out_ref[:, pl.ds(pl.multiple_of(block * width, width), width)] = piece.astype(jnp.bfloat16)
-    for j in range(n):
-        y_copy(j).wait_send()
+        return jnp.where(s == 0, z, jnp.where(d == 0, z - 1 - k, z + 1 + k))
+
+    wide = O.shape[5]
+    width = O.shape[1] * O.shape[4]
+
+    def rows_of(m, t):
+        return jnp.concatenate([M[m, t, k] for k in range(n)], axis=1)
+
+    def times(lhs, m, block):
+        weights = lambda t: O[block, :, t, m].reshape(width, wide)
+        return nt_dot(lhs[0], weights(0)) + nt_dot(lhs[1], weights(1))
+
+    def arrived(s):
+        block = order(s)
+        o = (z - block + n) % n
+        for kind in (C0, C1, C2, C3A, C3B):
+            piece = O.at[block, f, x, 0] if kind > C2 else O.at[block, f, x]
+            remote(piece, piece, o_send.at[kind, o], o_recv.at[kind, o], fs=core).wait_recv()
+        return block
+
+    with scope("mwait0"):
+        for flip, o in ways:
+            if flip or o:
+                m_copy(0, flip, o).wait_recv()
+            else:
+                m_copy(0, flip, o).wait()
+    lhs = [rows_of(0, t) for t in both]
+
+    def first_half(s, carry):
+        with scope("owait"):
+            block = arrived(s)
+        with scope("outp"):
+            acc[block] = times(lhs, 0, block)
+        return carry
+
+    lax.fori_loop(0, n, first_half, 0)
     for o in range(n):
-        for kind in range(3):
-            w_side(kind, o).wait_send()
+        for kind in range(KINDS):
+            o_side(kind, o).wait_send()
+    for flip, o in ways:
+        if flip or o:
+            m_copy(0, flip, o).wait_send()
+    t_copy(0).wait()
     for o in range(1, n):
         t_copy(o).wait()
-        e_copy(o).wait_send()
-        w_copy(o).wait_send()
-    for kind in range(3):
-        o_own(kind).wait_send()
-    for k in range(n - 1):
-        for d in both:
-            @pl.when(reach(d, k)[1])
-            def _(d=d, k=k):
-                for c in range(PARTS):
-                    xx_copy(d, k, c).wait_send()
-                for kind in range(3):
-                    o_side(kind, d, k).wait_send()
-
-            @pl.when(reach(d, k)[0])
-            def _(d=d, k=k):
-                for c in range(PARTS):
-                    x_copy(d, k, c).wait_send()
-                o_copy(d, k).wait_send()
+    for k in range(n):
+        T_ref[k : k + 1, :] = T[k, 0:1, :]
+    with scope("mwait1"):
+        for flip, o in ways:
+            if flip or o:
+                m_copy(1, flip, o).wait_recv()
+            else:
+                m_copy(1, flip, o).wait()
+    lhs2 = [rows_of(1, t) for t in both]
+
+    def put(block, s):
+        return pltpu.make_async_copy(
+            done.at[block], out_ref.at[:, pl.ds(pl.multiple_of(block * width, width), width)], out_sem.at[s]
+        )
+
+    def second_half(s, carry):
+        block = order(s)
+        done[block] = (acc[block] + times(lhs2, 1, block)).astype(jnp.bfloat16)
+        put(block, s).start()
+        return carry
+
+    with scope("outp2"):
+        lax.fori_loop(0, n, second_half, 0)
+    for flip, o in ways:
+        if flip or o:
+            m_copy(1, flip, o).wait_send()
+    with scope("put"):
+        for s in range(n):
+            put(order(s), s).wait()
 
 
 VMEM = pl.BlockSpec(memory_space=pltpu.VMEM)
+SMEM = pl.BlockSpec(memory_space=pltpu.SMEM)
 ANY = pl.BlockSpec(memory_space=pl.ANY)
 DMA = pltpu.SemaphoreType.DMA
 
@@ -704,51 +905,52 @@
     share, columns = query_weight_attention.shape
     width = 7 * HEAD
     half = tokens // 2
-    vectors = jnp.stack(
-        [jnp.broadcast_to(score_offset[:, None], (n, HEAD))]
-        + [
-            v.reshape(n, HEAD)
-            for v in (attention_norm_gain, recurrence_norm_gain, forget_floor, forget_offset)
-        ]
-    )
     bf = lambda *shape: pltpu.VMEM(shape, jnp.bfloat16)
     layer_out, T = pl.pallas_call(
         functools.partial(layer_kernel, n),
         out_shape=(
             jax.ShapeDtypeStruct((half, depth), jnp.bfloat16),
-            jax.ShapeDtypeStruct((n, 8, tokens), jnp.float32),
+            jax.ShapeDtypeStruct((n, tokens), jnp.float32),
         ),
-        in_specs=[VMEM] * 4 + [ANY] * 9,
-        out_specs=(VMEM,) * 2,
+        in_specs=[SMEM] + [VMEM] * 5 + [ANY] * 11,
+        out_specs=(ANY, VMEM),
         scratch_shapes=[
             bf(n, tokens, depth),
             bf(n, groups, share, width),
-            bf(n, groups, share, 2 * columns),
+            bf(n, groups, 2, 2, share, columns),
             bf(n, tokens, HEAD),
             bf(tokens, depth),
+            pltpu.VMEM((tokens, columns), jnp.float32),
             bf(tokens, columns),
             bf(n, share, width),
             bf(n * tokens, width),
             bf(n, tokens, HEAD),
             bf(n, tokens, HEAD),
             pltpu.VMEM((n, 8, tokens), jnp.float32),
-            bf(2, n, tokens, HEAD),
-            bf(n, half, depth // n),
+            pltpu.VMEM((n, 8, tokens), jnp.float32),
+            bf(2, 2, n, half, HEAD),
+            pltpu.VMEM((n, half, depth // n), jnp.float32),
             bf(n, half, depth // n),
         ]
         + [DMA((2, n, PARTS))] * 4
-        + [DMA((2, n))] * 2
-        + [DMA((3, n))] * 6
-        + [DMA((n,))] * 18
-        + [DMA((7, n)), DMA((8,))],
+        + [DMA((2, n, 2))] * 2
+        + [DMA((KINDS, n))] * 2
+        + [DMA((n,))] * 10
+        + [DMA((2, 2, n))] * 2
+        + [DMA((n,))] * 2
+        + [DMA((7, n)), DMA((8,)), DMA((n,))],
         compiler_params=pltpu.CompilerParams(
             collective_id=0, has_side_effects=True, vmem_limit_bytes=56 * 1024 * 1024
         ),
     )(
+        score_offset,
+        input_norm_gain[None],
+        attention_norm_gain[None],
+        recurrence_norm_gain[None],
+        forget_floor[None],
+        forget_offset[None],
         input_layer_rows[0],
-        input_norm_gain[None],
         extra_log_decay[0],
-        vectors,
         query_weight_attention,
         key_weight_attention,
         value_weight_attention,
@@ -759,7 +961,7 @@
         output_weight_attention,
         emitted_projection_linear_scan,
     )
-    return (layer_out[None], T[:, 0, :][None])
+    return (layer_out[None], T[None])
 
 
 def solution(mesh):

time: 123 us -> 108 us (0.88)
  Pallas kernels: 116 us -> 105 us
  local copies, waits for them, and re-layouts: 6.6 us -> 2.48 us
    pallas_call x1, Pallas kernels: 116 us -> 105 us  [on_device_heads(): pl.pallas_call(functools.partial(layer_kernel, n), out_shape=(jax.ShapeDt...]
    unnamed x18 -> x4, local copies, waits for them, and re-layouts: 5.83 us -> 2.48 us
where the time goes in v1:
time: 108 us
  Pallas kernels  105 us (97%)
  local copies, waits for them, and re-layouts  2.48 us (2%)
    pallas_call x1, Pallas kernels, on_device_heads(): pl.pallas_call(functools.partial(layer_kernel, n), out_shape=(jax.ShapeDt...  105 us
    unnamed x4, local copies, waits for them, and re-layouts  2.48 us

profile of v1, /device:TPU:0, one launch (start us, length us, event | category | flops | bytes accessed | tf_op | source)
XLA Modules:
  0.0 107.9 jit_solution(12624875862434647085)
XLA Ops:
  0.6 104.7 %shard_map.176 = (bf16[128,2048]{1,0:T(8,128)(2,1)}, f32[4,256]{1,0:T(4,128)}) custom-call(f32[4]{0:T(128)} %refs_0_.1, f32[1,2048]{1,0:T(1,128)} %bitcast.12, f32[1,512]{1,0:T(1,128)} %bitcast.14, f32[1,512]{1,0:T(1,128)} %bitcast.15, f32[1,512]{1,0:T(1,128)} %bitcast.16, f32[1,512]{1,0:T(1,128)} %bitcast.17, bf16[256,2048]{1,0:T(8,128)(2,1)} %bitcast.9, ...), custom_call_target="tpu_custom_call" | custom-call | tf_op jit(solution)/shard_map/pallas_call | solution.py:909
  105.4 0.0 copy-start
  105.4 1.9 %copy.21 = bf16[1,128,2048]{2,1,0:T(8,128)(2,1)} copy(bf16[1,128,2048]{2,1,0:T(8,128)(2,1)} %bitcast.10) | data formatting | bytes 1048576
  107.3 0.0 copy-done
  107.3 0.6 copy.22
Async XLA Ops:
  105.4 1.9 %copy-start = (f32[4,256]{1,0:T(4,128)S(1)}, f32[4,256]{1,0:T(4,128)}, u32[]{:S(2)}) copy-start(f32[4,256]{1,0:T(4,128)} %get-tuple-element.5) | copy-start | bytes 12292

commit v2 on v1

--- a/solution.py
+++ b/solution.py
@@ -335,12 +335,10 @@
     w_refs, o_refs = refs[8:15], refs[15:17]
     out_ref, T_ref = refs[17:19]
     (
-        X, W, O, E, raw_ref, xe_ref, e_ref, wp, proj, ma, mb, ts, T, M, acc, done,
-        x_send, x_recv, xx_send, xx_recv,
-        oz_send, oz_recv, o_send, o_recv,
-        w_send, w_recv, wy_send, wy_recv, wc_send, wc_recv, wd_send, wd_recv,
-        e_send, e_recv, m_send, m_recv, t_send, t_recv,
-        pack_sem, local_sem, out_sem,
+        X, W, O, E, raw_ref, xe_ref, e_ref, wp, proj, ma, mb, ts, T, M, acc,
+        x_send, x_recv, xx_send, xx_recv, oz_send, oz_recv, o_send, o_recv, oc_recv,
+        w_send, w_recv, wy_recv, ws_send, ws_recv, e_send, e_recv, m_send, m_recv, t_send, t_recv,
+        pack_sem, local_sem,
     ) = refs[19:]
     z, f, x = lax.axis_index("sp"), lax.axis_index("fs"), lax.axis_index("tp")
     core, row, side = f + 1 - 2 * (f % 2), (f + 2) % 4, 1 - x
@@ -362,7 +360,7 @@
         into = wp.at[o] if o else W.at[z, f]
         return [
             pltpu.make_async_copy(
-                w.at[:, cols((z + o) % n)], into.at[:, i * HEAD : (i + 1) * HEAD], pack_sem.at[i, o]
+                w.at[:, cols((z + o) % n)], into.at[:, i * HEAD : (i + 1) * HEAD], pack_sem.at[o]
             )
             for i, w in enumerate(w_refs)
         ]
@@ -373,10 +371,10 @@
 
     loads = [
         raw_half(x, 2),
-        raw_half(side, 5),
+        raw_half(side, 1),
         pltpu.make_async_copy(xe_hbm, xe_ref, local_sem.at[4]),
     ] + [
-        pltpu.make_async_copy(o, O.at[z, f, x, i], local_sem.at[i])
+        pltpu.make_async_copy(o, O.at[z, f, x, i], local_sem.at[0])
         for i, o in enumerate(o_refs)
     ]
     loads[0].start()
@@ -394,30 +392,32 @@
     def span(c):
         return pl.ds(pl.multiple_of(x * half + c * step, step), step)
 
-    def x_copy(direction, k, c):
+    def slot(direction, k):
+        return k + 1 if direction == 0 else n - 1 - k
+
+    def halves(which):
+        return pl.ds(pl.multiple_of(which * half, half), half)
+
+    def x_copy(direction, k, c, rows=None):
         _, _, out, _, to = reach(direction, k)
-        block = X.at[out, span(c)]
-        return remote(block, block, x_send.at[direction, k, c], x_recv.at[direction, k, c], sp=to)
+        block = X.at[out, span(c) if rows is None else rows]
+        return remote(block, block, x_send.at[direction, k], x_recv.at[slot(direction, k) - 1, c], sp=to)
 
     def x_wait(direction, k, c):
         block = X.at[reach(direction, k)[3], span(c)]
-        return remote(block, block, x_send.at[direction, k, c], x_recv.at[direction, k, c], sp=(z + 1) % n)
-
-    def xx_copy(direction, k, c):
-        block = X.at[reach(direction, k)[3], span(c)]
-        return remote(block, block, xx_send.at[direction, k, c], xx_recv.at[direction, k, c], tp=side)
-
-    def xx_wait(direction, k, c):
-        there = pl.ds(pl.multiple_of(side * half + c * step, step), step)
-        block = X.at[reach(direction, k)[3], there]
-        return remote(block, block, xx_send.at[direction, k, c], xx_recv.at[direction, k, c], tp=side)
+        return remote(block, block, x_send.at[direction, 0], x_recv.at[slot(direction, k) - 1, c], sp=(z + 1) % n)
+
+    def xx_copy(direction, k, rows):
+        o = slot(direction, k) - 1
+        block = X.at[reach(direction, k)[3], rows]
+        return remote(block, block, xx_send.at[o], xx_recv.at[o], tp=side)
 
     def o_copy(direction, k, m):
         _, _, out, _, to = reach(direction, k)
         piece = O.at[out, f, x, m]
-        return remote(piece, piece, oz_send.at[direction, k, m], oz_recv.at[direction, k, m], sp=to)
-
-    def o_side(kind, o):
+        return remote(piece, piece, oz_send.at[direction, k], oz_recv.at[slot(direction, k) - 1, m], sp=to)
+
+    def o_side(kind, o, by_y=False):
         block = (z - o + n) % n
         y, across, chip = {"fs": row}, {"tp": side}, {"fs": core}
         at, where = (
@@ -425,7 +425,7 @@
             ((f, x, 1), y),
             ((f, x, 0), across),
             ((f, x, 1), across),
-            ((row, x, 1), across),
+            ((f, side, 1), y) if by_y else ((row, x, 1), across),
             ((f, side, 0), y),
             ((f, x), chip),
             ((row, x), chip),
@@ -434,23 +434,23 @@
             ((row, side, 1), chip),
         )[kind]
         piece = O.at[(block, *at)]
-        return remote(piece, piece, o_send.at[kind, o], o_recv.at[kind, o], **where)
-
-    def slot(direction, k):
-        return k + 1 if direction == 0 else n - 1 - k
+        got = oc_recv.at[o] if kind >= C0 else o_recv.at[kind, o]
+        return remote(piece, piece, o_send.at[o], got, **where)
 
     def w_copy(o):
-        return remote(wp.at[o], W.at[z, f], w_send.at[o], w_recv.at[o], sp=(z + o) % n)
+        return remote(wp.at[o], W.at[z, f], w_send.at[0], w_recv.at[o], sp=(z + o) % n)
 
     def e_copy(o):
-        return remote(e_ref.at[:, cols((z + o) % n)], E.at[z], e_send.at[o], e_recv.at[o], sp=(z + o) % n)
+        return remote(e_ref.at[:, cols((z + o) % n)], E.at[z], e_send.at[0], e_recv.at[0], sp=(z + o) % n)
 
     def w_side(kind, o):
         block = (z - o + n) % n
         piece = W.at[block, row if kind == 2 else f]
-        send, recv = ((wy_send, wy_recv), (wc_send, wc_recv), (wd_send, wd_recv))[kind]
         where = {"fs": row if kind == 0 else core}
-        return remote(piece, piece, send.at[o], recv.at[o], **where)
+        return remote(piece, piece, ws_send.at[0], ws_recv.at[0] if kind else wy_recv.at[o], **where)
+
+    def local_wait(what, sem):
+        pltpu.make_async_copy(what, what, sem).wait()
 
     for copy in loads[1:3]:
         copy.start()
@@ -472,10 +472,9 @@
         lax.fori_loop(0, PARTS, normalise, x)
     with scope("packs"):
         for o in range(n):
-            for copy in packs(o):
-                copy.wait()
-    for copy in loads[3:]:
-        copy.wait()
+            into = wp.at[o] if o else W.at[z, f]
+            pltpu.make_async_copy(into, into, pack_sem.at[o]).wait()
+    pltpu.make_async_copy(O.at[z, f, x], O.at[z, f, x], local_sem.at[0]).wait()
     with scope("barrier"):
         pl.semaphore_wait(barrier, len(peers))
     o_begin(lambda at: (at == 0) | (at == n - 2))
@@ -517,7 +516,7 @@
         @pl.when(reach(d, k + 1)[0])
         def _():
             x_copy(d, k + 1, c).start()
-        xx_copy(d, k, c).start()
+        xx_copy(d, k, span(c)).start()
 
     def w_arrived(o):
         with scope("wz"):
@@ -532,7 +531,8 @@
 
     def o_pass(o, *pairs):
         for got, then in pairs:
-            o_side(got, o).wait_recv()
+            if got is not None:
+                o_side(got, o).wait_recv()
             o_side(then, o).start()
 
     def o_seen_x(o):
@@ -544,6 +544,14 @@
     def o_seen(o):
         o_seen_x(o)
         o_seen_y(o)
+
+    def o_by_y(d, k):
+        o = slot(d, k)
+        o_side(X1B, o).wait_recv()
+        o_side(X2, o, True).start()
+        for kind in (Y1B, Y1A):
+            o_side(kind, o).wait_recv()
+        o_side(C1, o).start()
 
     def o_across(o):
         o_pass(o, (X2, C3B), (Y2, C3A))
@@ -557,7 +565,7 @@
 
     def o_half(d, k, m, kinds, relay=True):
         piece = O.at[reach(d, k)[3], f, x, m]
-        remote(piece, piece, oz_send.at[d, k, m], oz_recv.at[d, k, m], sp=(z + 1) % n).wait_recv()
+        remote(piece, piece, oz_send.at[d, k], oz_recv.at[slot(d, k) - 1, m], sp=(z + 1) % n).wait_recv()
         if relay:
             o_relay(d, k, (m,))
         for kind in kinds:
@@ -645,9 +653,7 @@
 
     outer = (z == 0) | (z == n - 1)
     with scope("wc"):
-        for o in range(n):
-            w_side(1, o).wait_recv()
-            w_side(2, o).wait_recv()
+        local_wait(W.at[0:2], ws_recv.at[0])
 
     def gather_step(k, carry):
         @pl.when(k == 1)
@@ -659,28 +665,34 @@
         def _():
             with scope("o21"):
                 each(1, lambda at: at == 2, o_full)
-            each(1, lambda at: at > 2, lambda d, k: o_side(X1A, slot(d, k)).start())
             with scope("look31"):
-                each(1, lambda at: at > 2, lambda d, k: o_seen_y(slot(d, k)))
-
-        pl.when((k == 2) & outer)(e_begin)
-        pl.when((k == 3) & jnp.logical_not(outer))(e_begin)
+                each(1, lambda at: at > 2, o_by_y)
+
+        pl.when((k == n - 1) & outer)(e_begin)
 
         @pl.when(z - k >= 0)
         def _():
             @pl.when(k > 0)
             def _():
-                for c in range(PARTS):
-                    with scope("xx"):
-                        xx_wait(0, k - 1, c).wait_recv()
+                with scope("xx"):
+                    xx_copy(0, k - 1, halves(side)).wait_recv()
+
+            @pl.when(k == n - 1)
+            def _():
+                o_side(X1A, slot(0, 1)).start()
+
             with scope("proj"):
                 project(z - k)
 
         @pl.when((k > 0) & (z + k < n))
         def _():
-            for c in range(PARTS):
-                with scope("xx"):
-                    xx_wait(1, k - 1, c).wait_recv()
+            with scope("xx"):
+                xx_copy(1, k - 1, halves(side)).wait_recv()
+
+            @pl.when(k == n - 1)
+            def _():
+                o_side(X1A, slot(1, 1)).start()
+
             with scope("proj"):
                 project(z + k)
 
@@ -698,15 +710,14 @@
         to = side if flip else x
         rows = pl.ds(pl.multiple_of(to * half, half), half)
         src = (ma, mb)[m].at[(z + o) % n, rows]
-        sems = m_send.at[m, flip, o], m_recv.at[m, flip, o]
         if o == 0 and not flip:
-            return pltpu.make_async_copy(src, M.at[m, x, z], sems[1])
-        return remote(src, M.at[m, x, z], *sems, sp=(z + o) % n, tp=to)
+            return pltpu.make_async_copy(src, M.at[m, x, z], m_recv.at[m])
+        return remote(src, M.at[m, x, z], m_send.at[0], m_recv.at[m], sp=(z + o) % n, tp=to)
 
     def t_copy(o):
         if o == 0:
-            return pltpu.make_async_copy(ts.at[z], T.at[z], t_recv.at[o])
-        return remote(ts.at[(z + o) % n], T.at[z], t_send.at[o], t_recv.at[o], sp=(z + o) % n)
+            return pltpu.make_async_copy(ts.at[z], T.at[z], t_recv.at[0])
+        return remote(ts.at[(z + o) % n], T.at[z], t_send.at[0], t_recv.at[0], sp=(z + o) % n)
 
     ways = [(flip, o) for o in range(n - 1, -1, -1) for flip in both]
 
@@ -718,35 +729,44 @@
         ma[i] = mixed
         total = jnp.log(jnp.maximum(1.0 - jnp.exp(keep), log_floor))
         ts[i] = jnp.broadcast_to(total, (tokens, HEAD)).T[0:8, :]
-    with scope("o32"):
-        each(2, always, o_first)
+        if i == 0:
+            pl.when(jnp.logical_not(outer))(e_begin)
+        if i == 0:
+            with scope("o32"):
+                each(2, always, o_first)
+        if i == min(2, n - 1):
+            with scope("o33"):
+                each(2, always, o_second)
     local[1].wait()
     with scope('ewait'):
-        for o in range(1, n):
-            e_copy(o).wait_recv()
+        local_wait(E.at[1:n], e_recv.at[0])
     floor, offset, gain = param(2), param(3), param(1)
     per = tokens // CHUNK
 
-    def tick0():
-        each(2, always, o_second)
-        each(1, lambda at: at > 2, lambda d, k: o_seen_x(slot(d, k)))
-
-    def tick1():
-        each(1, lambda at: at == 2, look)
-
-    def tick3():
+    def a_begin():
         for way in ways:
             m_copy(0, *way).start()
         for o in range(n):
             t_copy(o).start()
 
+    def tick1():
+        each(1, lambda at: at > 2, lambda d, k: o_pass(slot(d, k), (X1A, Y2), (None, C2)))
+        each(2, always, lambda d, k: o_pass(slot(d, k), (Y1B, X2)))
+        each(1, lambda at: at == 2, look)
+
+    def tick3():
+        a_begin()
+
     def tick5():
+        each(1, lambda at: at == 2, over)
+        each(2, always, lambda d, k: o_pass(slot(d, k), (X1A, Y2), (X1B, C2)))
+
+    def tick6():
+        each(2, always, lambda d, k: o_pass(slot(d, k), (Y1A, C1)))
         each(1, lambda at: at > 2, over)
-        each(1, lambda at: at == 2, over)
-        each(2, always, lambda d, k: o_seen_x(slot(d, k)))
 
     count = per * n
-    ticks = ((0, tick0), (1, tick1), (3, tick3), (5, tick5))
+    ticks = ((1, tick1), (3, tick3), (5, tick5), (6, tick6))
 
     def chunk(i, state):
         here = pl.ds(pl.multiple_of(i * CHUNK, CHUNK), CHUNK)
@@ -766,32 +786,6 @@
         lax.fori_loop(0, count, chunk, state)
     for way in ways:
         m_copy(1, *way).start()
-    with scope("end2"):
-        each(2, always, lambda d, k: o_seen_y(slot(d, k)))
-    with scope("end3"):
-        each(2, always, over)
-
-    with scope("drain"):
-        for o in range(n):
-            for kind in range(3):
-                w_side(kind, o).wait_send()
-        for o in range(1, n):
-            e_copy(o).wait_send()
-            w_copy(o).wait_send()
-        for k in range(n - 1):
-            for d in both:
-                @pl.when(reach(d, k)[1])
-                def _(d=d, k=k):
-                    for c in range(PARTS):
-                        xx_copy(d, k, c).wait_send()
-
-                @pl.when(reach(d, k)[0])
-                def _(d=d, k=k):
-                    for c in range(PARTS):
-                        x_copy(d, k, c).wait_send()
-                    for m in both:
-                        o_copy(d, k, m).wait_send()
-
     def order(s):
         shorter = jnp.minimum(z, n - 1 - z)
         t = s - 1
@@ -813,17 +807,11 @@
     def arrived(s):
         block = order(s)
         o = (z - block + n) % n
-        for kind in (C0, C1, C2, C3A, C3B):
-            piece = O.at[block, f, x, 0] if kind > C2 else O.at[block, f, x]
-            remote(piece, piece, o_send.at[kind, o], o_recv.at[kind, o], fs=core).wait_recv()
+        local_wait(O.at[block, 0:2], oc_recv.at[o])
         return block
 
     with scope("mwait0"):
-        for flip, o in ways:
-            if flip or o:
-                m_copy(0, flip, o).wait_recv()
-            else:
-                m_copy(0, flip, o).wait()
+        local_wait(M.at[0], m_recv.at[0])
     lhs = [rows_of(0, t) for t in both]
 
     def first_half(s, carry):
@@ -833,45 +821,45 @@
             acc[block] = times(lhs, 0, block)
         return carry
 
-    lax.fori_loop(0, n, first_half, 0)
+    lax.fori_loop(0, n - 1, first_half, 0)
+    with scope("end3"):
+        each(2, always, over)
+    with scope("drain"):
+        local_wait(W.at[1:n], ws_send.at[0])
+        local_wait(wp.at[1:n], w_send.at[0])
+        local_wait(E.at[1:n], e_send.at[0])
+        for k in range(n - 1):
+            for d in both:
+                @pl.when(reach(d, k)[1])
+                def _(d=d, k=k):
+                    xx_copy(d, k, halves(x)).wait_send()
+
+                @pl.when(reach(d, k)[0])
+                def _(d=d, k=k):
+                    x_copy(d, k, 0, halves(x)).wait_send()
+                    whole = O.at[z, f, x]
+                    remote(whole, whole, oz_send.at[d, k], oz_recv.at[0, 0], sp=(z + 1) % n).wait_send()
+
+    lax.fori_loop(n - 1, n, first_half, 0)
     for o in range(n):
-        for kind in range(KINDS):
-            o_side(kind, o).wait_send()
-    for flip, o in ways:
-        if flip or o:
-            m_copy(0, flip, o).wait_send()
-    t_copy(0).wait()
-    for o in range(1, n):
-        t_copy(o).wait()
+        local_wait(proj, o_send.at[o])
+    local_wait(T, t_recv.at[0])
+    local_wait(T.at[1:n], t_send.at[0])
     for k in range(n):
         T_ref[k : k + 1, :] = T[k, 0:1, :]
     with scope("mwait1"):
-        for flip, o in ways:
-            if flip or o:
-                m_copy(1, flip, o).wait_recv()
-            else:
-                m_copy(1, flip, o).wait()
+        local_wait(M.at[1], m_recv.at[1])
     lhs2 = [rows_of(1, t) for t in both]
-
-    def put(block, s):
-        return pltpu.make_async_copy(
-            done.at[block], out_ref.at[:, pl.ds(pl.multiple_of(block * width, width), width)], out_sem.at[s]
-        )
 
     def second_half(s, carry):
         block = order(s)
-        done[block] = (acc[block] + times(lhs2, 1, block)).astype(jnp.bfloat16)
-        put(block, s).start()
+        at = pl.ds(pl.multiple_of(block * width, width), width)
+        out_ref[:, at] = (acc[block] + times(lhs2, 1, block)).astype(jnp.bfloat16)
         return carry
 
     with scope("outp2"):
         lax.fori_loop(0, n, second_half, 0)
-    for flip, o in ways:
-        if flip or o:
-            m_copy(1, flip, o).wait_send()
-    with scope("put"):
-        for s in range(n):
-            put(order(s), s).wait()
+    local_wait(wp.at[0:2], m_send.at[0])
 
 
 VMEM = pl.BlockSpec(memory_space=pltpu.VMEM)
@@ -909,11 +897,11 @@
     layer_out, T = pl.pallas_call(
         functools.partial(layer_kernel, n),
         out_shape=(
-            jax.ShapeDtypeStruct((half, depth), jnp.bfloat16),
-            jax.ShapeDtypeStruct((n, tokens), jnp.float32),
+            pltpu.VMEM((half, depth), jnp.bfloat16),
+            pltpu.VMEM((n, tokens), jnp.float32),
         ),
         in_specs=[SMEM] + [VMEM] * 5 + [ANY] * 11,
-        out_specs=(ANY, VMEM),
+        out_specs=(VMEM, VMEM),
         scratch_shapes=[
             bf(n, tokens, depth),
             bf(n, groups, share, width),
@@ -930,15 +918,12 @@
             pltpu.VMEM((n, 8, tokens), jnp.float32),
             bf(2, 2, n, half, HEAD),
             pltpu.VMEM((n, half, depth // n), jnp.float32),
-            bf(n, half, depth // n),
         ]
-        + [DMA((2, n, PARTS))] * 4
-        + [DMA((2, n, 2))] * 2
-        + [DMA((KINDS, n))] * 2
-        + [DMA((n,))] * 10
-        + [DMA((2, 2, n))] * 2
-        + [DMA((n,))] * 2
-        + [DMA((7, n)), DMA((8,)), DMA((n,))],
+        + [DMA((2, n - 1)), DMA((n - 1, PARTS)), DMA((n - 1,)), DMA((n - 1,))]
+        + [DMA((2, n - 1)), DMA((n - 1, 2)), DMA((n,)), DMA((C0, n)), DMA((n,))]
+        + [DMA((1,)), DMA((n,)), DMA((n,)), DMA((1,)), DMA((1,))]
+        + [DMA((1,)), DMA((1,)), DMA((1,)), DMA((2,)), DMA((1,)), DMA((1,))]
+        + [DMA((n,)), DMA((5,))],
         compiler_params=pltpu.CompilerParams(
             collective_id=0, has_side_effects=True, vmem_limit_bytes=56 * 1024 * 1024
         ),

time: 108 us -> 98.4 us (0.911)
  Pallas kernels: 105 us -> 96.2 us
  local copies, waits for them, and re-layouts: 2.48 us -> 1.39 us
    pallas_call x1, Pallas kernels: 105 us -> 96.2 us  [on_device_heads(): pl.pallas_call(functools.partial(layer_kernel, n), out_shape=(pltpu.VMEM(...]
    unnamed x4 -> x2, local copies, waits for them, and re-layouts: 2.48 us -> 1.39 us
where the time goes in v2:
time: 98.4 us; the launch traced here: 98.2 us
  Pallas kernels  96.2 us (98%)
  local copies, waits for them, and re-layouts  1.39 us (1%)
    pallas_call x1, Pallas kernels, on_device_heads(): pl.pallas_call(functools.partial(layer_kernel, n), out_shape=(pltpu.VMEM(...  96.2 us

profile of v2, /device:TPU:0, one launch (start us, length us, event | category | flops | bytes accessed | tf_op | source)
XLA Modules:
  0.0 98.2 jit_solution(7756806809163466996)
XLA Ops:
  0.6 96.2 %shard_map.176 = (bf16[128,2048]{1,0:T(8,128)(2,1)S(1)}, f32[4,256]{1,0:T(4,128)S(1)}) custom-call(f32[4]{0:T(128)} %refs_0_.1, f32[1,2048]{1,0:T(1,128)} %bitcast.13, f32[1,512]{1,0:T(1,128)} %bitcast.14, f32[1,512]{1,0:T(1,128)} %bitcast.15, f32[1,512]{1,0:T(1,128)} %bitcast.16, f32[1,512]{1,0:T(1,128)} %bitcast.17, bf16[256,2048]{1,0:T(8,128)(2,1)} %bitcast.11, ...), custom_call_target="tpu_custom_call" | custom-call | tf_op jit(solution)/shard_map/pallas_call | solution.py:897
  96.8 0.8 copy.21
  97.6 0.6 copy.22

commit v3 on v2

--- a/solution.py
+++ b/solution.py
@@ -228,7 +228,6 @@
     return (layer_out, row_log_total)
 
 
-LEAF = 16
 CHUNK = 128
 TILE = 256
 MESH = pl.DeviceIdType.MESH
@@ -288,9 +287,27 @@
     return head_norm(total, gain).astype(jnp.bfloat16), keep
 
 
+def prefix_sums(lower, values):
+    total = jnp.zeros(values.shape, jnp.float32)
+    for _ in range(3):
+        piece = values.astype(jnp.bfloat16)
+        total += jnp.dot(lower, piece, preferred_element_type=jnp.float32)
+        values = values - piece.astype(jnp.float32)
+    return total
+
+
+def boundaries(run, r, size):
+    row = lambda at, count: jnp.broadcast_to(run[at : at + 1, :], (count, run.shape[1]))
+    if size > 2:
+        return jnp.concatenate([row(b + size - 1, 2 * size) for b in range(0, CHUNK, 2 * size)], axis=0)
+    first = jnp.concatenate([row(b + 1, 8) for b in range(0, CHUNK, 8)], axis=0)
+    second = jnp.concatenate([row(b + 5, 8) for b in range(0, CHUNK, 8)], axis=0)
+    return jnp.where(r % 8 < 4, first, second)
+
+
 def recur_chunk(p_ref, e_ref, here, state, floor, offset, gain):
     r, c = grid_of((CHUNK, CHUNK))
-    lower = (r >= c).astype(jnp.float32)
+    lower = (r >= c).astype(jnp.bfloat16)
     part = lambda k: p_ref[here, k * HEAD : (k + 1) * HEAD].astype(jnp.float32)
     raw = part(3)
     query = raw * jax.nn.sigmoid(raw)
@@ -298,20 +315,23 @@
     value = p_ref[here, 5 * HEAD : 6 * HEAD]
     gate = part(6)
     decay = jnp.log1p(-key) + e_ref[...].astype(jnp.float32)
-    run = jnp.dot(lower, decay, precision=lax.Precision.HIGHEST, preferred_element_type=jnp.float32)
-    stripes = [jnp.zeros((LEAF, CHUNK), jnp.float32)]
-    for s in range(LEAF, CHUNK, LEAF):
-        edge = run[s - 1 : s, :]
-        near = (query[s : s + LEAF] * jnp.exp(run[s : s + LEAF] - edge)).astype(jnp.bfloat16)
-        far = (key * jnp.exp(jnp.where(r < s, edge - run, -jnp.inf))).astype(jnp.bfloat16)
-        stripes.append(nt_dot(near, far))
-    pairs = jnp.concatenate(stripes, axis=0)
-    for d in range(LEAF):
-        back_key = pltpu.roll(key, d, 0) if d else key
-        back_run = pltpu.roll(run, d, 0) if d else run
-        gap = jnp.where(r % LEAF >= d, run - back_run, -jnp.inf)
-        column = jnp.sum(query * back_key * jnp.exp(gap), axis=1, keepdims=True)
-        pairs = jnp.where((r - c == d) & (r % LEAF >= d), column, pairs)
+    run = prefix_sums(lower, decay)
+    apart = r ^ c
+    pairs = jnp.where(r == c, jnp.sum(query * key, axis=1, keepdims=True), 0.0)
+    size = 1
+    while size < CHUNK:
+        later = (r & size) != 0
+        if size == 1:
+            reach = jnp.where(later, decay, 0.0)
+        else:
+            gap = run - boundaries(run, r, size)
+            reach = jnp.where(later, gap, -gap)
+        scale = jnp.exp(reach)
+        near = (query * scale).astype(jnp.bfloat16)
+        far = (key * scale).astype(jnp.bfloat16)
+        pairs = jnp.where(apart >= size, nt_dot(near, far), pairs)
+        size *= 2
+    pairs = jnp.where(r >= c, pairs, 0.0)
     last = run[CHUNK - 1 : CHUNK, :]
     out = jnp.dot(pairs.astype(jnp.bfloat16), value, preferred_element_type=jnp.float32)
     out += nt_dot((query * jnp.exp(run)).astype(jnp.bfloat16), state.astype(jnp.bfloat16))
@@ -377,13 +397,12 @@
         pltpu.make_async_copy(o, O.at[z, f, x, i], local_sem.at[0])
         for i, o in enumerate(o_refs)
     ]
-    loads[0].start()
     for copy in loads[3:]:
         copy.start()
+    loads[0].start()
     for o in range(n - 1, -1, -1):
         for copy in packs(o):
             copy.start()
-
     def reach(direction, k):
         if direction == 0:
             return (z - k >= 0) & (z + 1 < n), z - 1 - k >= 0, z - k, z - 1 - k, z + 1
@@ -452,14 +471,6 @@
     def local_wait(what, sem):
         pltpu.make_async_copy(what, what, sem).wait()
 
-    for copy in loads[1:3]:
-        copy.start()
-
-    def normalise(i, which):
-        rows = pl.ds(pl.multiple_of(which * half + i * step, step), step)
-        X[z, rows, :] = head_norm(raw_ref[rows, :].astype(jnp.float32), g_ref[...]).astype(jnp.bfloat16)
-        return which
-
     def o_begin(when):
         for d in both:
             @pl.when(when(z if d == 0 else n - 1 - z))
@@ -467,22 +478,30 @@
                 for m in (1, 0):
                     o_copy(d, 0, m).start()
 
+    for copy in loads[1:3]:
+        copy.start()
+    with scope("barrier"):
+        pl.semaphore_wait(barrier, len(peers))
+    pltpu.make_async_copy(O.at[z, f, x], O.at[z, f, x], local_sem.at[0]).wait()
+    o_begin(lambda at: (at == 0) | (at == n - 2))
+
+    def normalise(i, which):
+        rows = pl.ds(pl.multiple_of(which * half + i * step, step), step)
+        X[z, rows, :] = head_norm(raw_ref[rows, :].astype(jnp.float32), g_ref[...]).astype(jnp.bfloat16)
+        return which
+
     loads[0].wait()
     with scope("norm"):
         lax.fori_loop(0, PARTS, normalise, x)
-    with scope("packs"):
-        for o in range(n):
-            into = wp.at[o] if o else W.at[z, f]
-            pltpu.make_async_copy(into, into, pack_sem.at[o]).wait()
-    pltpu.make_async_copy(O.at[z, f, x], O.at[z, f, x], local_sem.at[0]).wait()
-    with scope("barrier"):
-        pl.semaphore_wait(barrier, len(peers))
-    o_begin(lambda at: (at == 0) | (at == n - 2))
     for d in both:
         @pl.when(reach(d, 0)[0])
         def _(d=d):
             for c in range(PARTS):
                 x_copy(d, 0, c).start()
+    with scope("packs"):
+        for o in range(n):
+            into = wp.at[o] if o else W.at[z, f]
+            pltpu.make_async_copy(into, into, pack_sem.at[o]).wait()
     for far in range(n - 1, 0, -1):
         @pl.when(z + far < n)
         def _(far=far):
@@ -533,7 +552,8 @@
         for got, then in pairs:
             if got is not None:
                 o_side(got, o).wait_recv()
-            o_side(then, o).start()
+            if then is not None:
+                o_side(then, o).start()
 
     def o_seen_x(o):
         o_pass(o, (X1A, Y2), (X1B, C2))
@@ -546,12 +566,14 @@
         o_seen_y(o)
 
     def o_by_y(d, k):
-        o = slot(d, k)
-        o_side(X1B, o).wait_recv()
-        o_side(X2, o, True).start()
-        for kind in (Y1B, Y1A):
-            o_side(kind, o).wait_recv()
-        o_side(C1, o).start()
+        o_side(X1B, slot(d, k)).wait_recv()
+        o_side(X2, slot(d, k), True).start()
+
+    def o_got_y(d, k):
+        o_pass(slot(d, k), (Y1B, None), (Y1A, C1))
+
+    def o_got_x(d, k):
+        o_pass(slot(d, k), (X1A, Y2), (None, C2))
 
     def o_across(o):
         o_pass(o, (X2, C3B), (Y2, C3A))
@@ -663,10 +685,14 @@
 
         @pl.when(k == n - 1)
         def _():
+            with scope("look31"):
+                each(1, lambda at: at > 2, o_by_y)
+                each(1, lambda at: at > 2, o_got_y)
+
+        @pl.when(k == n - 2)
+        def _():
             with scope("o21"):
                 each(1, lambda at: at == 2, o_full)
-            with scope("look31"):
-                each(1, lambda at: at > 2, o_by_y)
 
         pl.when((k == n - 1) & outer)(e_begin)
 
@@ -703,6 +729,8 @@
 
     x_hop(2, 0)
     lax.fori_loop(0, n, gather_step, 0)
+    with scope("o32"):
+        each(2, always, o_first)
     with scope("over0"):
         each(0, lambda at: at == 2, over)
 
@@ -729,14 +757,12 @@
         ma[i] = mixed
         total = jnp.log(jnp.maximum(1.0 - jnp.exp(keep), log_floor))
         ts[i] = jnp.broadcast_to(total, (tokens, HEAD)).T[0:8, :]
-        if i == 0:
+        if i == min(2, n - 1):
             pl.when(jnp.logical_not(outer))(e_begin)
-        if i == 0:
-            with scope("o32"):
-                each(2, always, o_first)
         if i == min(2, n - 1):
             with scope("o33"):
                 each(2, always, o_second)
+                each(1, lambda at: at > 2, o_got_x)
     local[1].wait()
     with scope('ewait'):
         local_wait(E.at[1:n], e_recv.at[0])
@@ -749,31 +775,32 @@
         for o in range(n):
             t_copy(o).start()
 
+    def tick0():
+        each(2, always, o_by_y)
+        each(1, lambda at: at == 2, look)
+
     def tick1():
-        each(1, lambda at: at > 2, lambda d, k: o_pass(slot(d, k), (X1A, Y2), (None, C2)))
-        each(2, always, lambda d, k: o_pass(slot(d, k), (Y1B, X2)))
-        each(1, lambda at: at == 2, look)
-
-    def tick3():
-        a_begin()
+        pl.when(jnp.logical_not(outer))(a_begin)
+        each(2, always, o_got_y)
+
+    def tick2():
+        each(2, always, o_got_x)
 
     def tick5():
         each(1, lambda at: at == 2, over)
-        each(2, always, lambda d, k: o_pass(slot(d, k), (X1A, Y2), (X1B, C2)))
 
     def tick6():
-        each(2, always, lambda d, k: o_pass(slot(d, k), (Y1A, C1)))
         each(1, lambda at: at > 2, over)
 
-    count = per * n
-    ticks = ((1, tick1), (3, tick3), (5, tick5), (6, tick6))
-
-    def chunk(i, state):
-        here = pl.ds(pl.multiple_of(i * CHUNK, CHUNK), CHUNK)
-        at = pl.ds(pl.multiple_of((i % per) * CHUNK, CHUNK), CHUNK)
-        extra = E.at[i // per, at]
-        mixed, state = recur_chunk(proj, extra, here, state, floor, offset, gain)
-        mb[i // per, at, :] = mixed
+    pl.when(outer)(a_begin)
+    ticks = ((0, tick0), (1, tick1), (2, tick2))
+
+    def recur_block(i, state):
+        for j in range(per):
+            here = pl.ds(pl.multiple_of(i * tokens + j * CHUNK, CHUNK), CHUNK)
+            at = slice(j * CHUNK, (j + 1) * CHUNK)
+            mixed, state = recur_chunk(proj, E.at[i, at], here, state, floor, offset, gain)
+            mb[i, at, :] = mixed
         for when, tick in ticks:
             @pl.when(i == when)
             def _(when=when, tick=tick):
@@ -783,9 +810,12 @@
 
     state = jnp.zeros((HEAD, HEAD), jnp.float32)
     with scope("rec"):
-        lax.fori_loop(0, count, chunk, state)
+        lax.fori_loop(0, n, recur_block, state)
     for way in ways:
         m_copy(1, *way).start()
+    with scope("passes"):
+        tick5()
+        tick6()
     def order(s):
         shorter = jnp.minimum(z, n - 1 - z)
         t = s - 1
@@ -851,14 +881,11 @@
         local_wait(M.at[1], m_recv.at[1])
     lhs2 = [rows_of(1, t) for t in both]
 
-    def second_half(s, carry):
-        block = order(s)
-        at = pl.ds(pl.multiple_of(block * width, width), width)
-        out_ref[:, at] = (acc[block] + times(lhs2, 1, block)).astype(jnp.bfloat16)
-        return carry
-
     with scope("outp2"):
-        lax.fori_loop(0, n, second_half, 0)
+        for s in range(n):
+            block = order(s)
+            at = pl.ds(pl.multiple_of(block * width, width), width)
+            out_ref[:, at] = (acc[block] + times(lhs2, 1, block)).astype(jnp.bfloat16)
     local_wait(wp.at[0:2], m_send.at[0])
 
 

time: 98.4 us -> 96.1 us (0.977)
  Pallas kernels: 96.2 us -> 93.9 us
    pallas_call x1, Pallas kernels: 96.2 us -> 93.9 us  [on_device_heads(): pl.pallas_call(functools.partial(layer_kernel, n), out_shape=(pltpu.VMEM(...]
where the time goes in v3:
time: 96.1 us; the launch traced here: 96 us
  Pallas kernels  93.9 us (98%)
  local copies, waits for them, and re-layouts  1.39 us (1%)
    pallas_call x1, Pallas kernels, on_device_heads(): pl.pallas_call(functools.partial(layer_kernel, n), out_shape=(pltpu.VMEM(...  93.9 us

profile of v3, /device:TPU:0, one launch (start us, length us, event | category | flops | bytes accessed | tf_op | source)
XLA Modules:
  0.0 96.0 jit_solution(12189870367958136434)
XLA Ops:
  0.6 93.9 %shard_map.176 = (bf16[128,2048]{1,0:T(8,128)(2,1)S(1)}, f32[4,256]{1,0:T(4,128)S(1)}) custom-call(f32[4]{0:T(128)} %refs_0_.1, f32[1,2048]{1,0:T(1,128)} %bitcast.13, f32[1,512]{1,0:T(1,128)} %bitcast.14, f32[1,512]{1,0:T(1,128)} %bitcast.15, f32[1,512]{1,0:T(1,128)} %bitcast.16, f32[1,512]{1,0:T(1,128)} %bitcast.17, bf16[256,2048]{1,0:T(8,128)(2,1)} %bitcast.11, ...), custom_call_target="tpu_custom_call" | custom-call | tf_op jit(solution)/shard_map/pallas_call | solution.py:924
  94.6 0.8 copy.21
  95.4 0.6 copy.22

commit v4 on v3

--- a/solution.py
+++ b/solution.py
@@ -258,33 +258,27 @@
     return lax.broadcasted_iota(jnp.int32, shape, 0), lax.broadcasted_iota(jnp.int32, shape, 1)
 
 
-def attend_tile(i, p_ref, shift, gain):
-    here = slice(i * TILE, (i + 1) * TILE)
+def attend_tile(p_ref, i, j, diagonal, shift, carry):
     r, c = grid_of((TILE, TILE))
     later = (r > c).astype(jnp.bfloat16)
-    query = p_ref[here, 0:HEAD]
-    total = jnp.zeros((TILE, HEAD), jnp.float32)
-    keep = jnp.zeros((TILE, 1), jnp.float32)
-    for j in range(i, -1, -1):
-        there = slice(j * TILE, (j + 1) * TILE)
-        score = nt_dot(query, p_ref[there, HEAD : 2 * HEAD]) * HEAD ** (-0.5) + shift
-        soft = -(jnp.maximum(score, 0.0) + jnp.log1p(jnp.exp(-jnp.abs(score))))
-        held = jnp.where(r > c, soft, 0.0) if i == j else soft
-        high = held.astype(jnp.bfloat16)
-        low = (held - high.astype(jnp.float32)).astype(jnp.bfloat16)
-        suffix = jnp.dot(high, later, preferred_element_type=jnp.float32) + jnp.dot(
-            low, later, preferred_element_type=jnp.float32
-        )
-        weight = jnp.exp(score + soft + suffix + keep)
-        if i == j:
-            weight = jnp.where(r > c, weight, 0.0)
-        total += jnp.dot(
-            weight.astype(jnp.bfloat16),
-            p_ref[there, 2 * HEAD : 3 * HEAD],
-            preferred_element_type=jnp.float32,
-        )
-        keep += jnp.sum(held, axis=1, keepdims=True)
-    return head_norm(total, gain).astype(jnp.bfloat16), keep
+    rows = lambda at: pl.ds(pl.multiple_of(at * TILE, TILE), TILE)
+    total, keep = carry
+    query = p_ref[rows(i), 0:HEAD]
+    score = nt_dot(query, p_ref[rows(j), HEAD : 2 * HEAD]) * HEAD ** (-0.5) + shift
+    soft = -(jnp.maximum(score, 0.0) + jnp.log1p(jnp.exp(-jnp.abs(score))))
+    held = jnp.where(r > c, soft, 0.0) if diagonal else soft
+    high = held.astype(jnp.bfloat16)
+    low = (held - high.astype(jnp.float32)).astype(jnp.bfloat16)
+    suffix = jnp.dot(high, later, preferred_element_type=jnp.float32) + jnp.dot(
+        low, later, preferred_element_type=jnp.float32
+    )
+    weight = jnp.exp(score + soft + suffix + keep)
+    if diagonal:
+        weight = jnp.where(r > c, weight, 0.0)
+    total += jnp.dot(
+        weight.astype(jnp.bfloat16), p_ref[rows(j), 2 * HEAD : 3 * HEAD], preferred_element_type=jnp.float32
+    )
+    return total, keep + jnp.sum(held, axis=1, keepdims=True)
 
 
 def prefix_sums(lower, values):
@@ -340,7 +334,8 @@
     return mixed.astype(jnp.bfloat16), state
 
 
-PARTS = 4
+PARTS = 8
+PAIR = 2
 Y1A, Y1B, X1A, X1B, X2, Y2, C0, C1, C2, C3A, C3B = range(11)
 KINDS = 11
 OPEN = (Y1B, X1B, X1A, Y1A, C0)
@@ -350,15 +345,15 @@
 
 
 def layer_kernel(n, *refs):
-    s_ref, g_ref, v_refs = refs[0], refs[1], refs[2:6]
+    s_ref, small = refs[0], refs[1:6]
     raw_hbm, xe_hbm = refs[6:8]
     w_refs, o_refs = refs[8:15], refs[15:17]
     out_ref, T_ref = refs[17:19]
     (
-        X, W, O, E, raw_ref, xe_ref, e_ref, wp, proj, ma, mb, ts, T, M, acc,
+        X, W, O, E, raw_ref, xe_ref, e_ref, wp, proj, ma, mb, ts, T, M, acc, g_ref, v_ref, at_total, at_keep, R,
         x_send, x_recv, xx_send, xx_recv, oz_send, oz_recv, o_send, o_recv, oc_recv,
         w_send, w_recv, wy_recv, ws_send, ws_recv, e_send, e_recv, m_send, m_recv, t_send, t_recv,
-        pack_sem, local_sem,
+        pack_sem, local_sem, small_sem, r_send, r_recv,
     ) = refs[19:]
     z, f, x = lax.axis_index("sp"), lax.axis_index("fs"), lax.axis_index("tp")
     core, row, side = f + 1 - 2 * (f % 2), (f + 2) % 4, 1 - x
@@ -389,6 +384,10 @@
         rows = pl.ds(pl.multiple_of(which * half, half), half)
         return pltpu.make_async_copy(raw_hbm.at[rows], raw_ref.at[rows], local_sem.at[sem])
 
+    smalls = [
+        pltpu.make_async_copy(ref, g_ref if i == 0 else v_ref.at[pl.ds(i - 1, 1)], small_sem.at[i])
+        for i, ref in enumerate(small)
+    ]
     loads = [
         raw_half(x, 2),
         raw_half(side, 1),
@@ -400,6 +399,8 @@
     for copy in loads[3:]:
         copy.start()
     loads[0].start()
+    for copy in smalls:
+        copy.start()
     for o in range(n - 1, -1, -1):
         for copy in packs(o):
             copy.start()
@@ -491,6 +492,8 @@
         return which
 
     loads[0].wait()
+    for copy in smalls:
+        copy.wait()
     with scope("norm"):
         lax.fori_loop(0, PARTS, normalise, x)
     for d in both:
@@ -629,12 +632,13 @@
             def _(o=far if d == 0 else n - far):
                 do(o)
 
-    def x_hop(k, c):
-        for d in both:
-            @pl.when(reach(d, k)[1])
-            def _(d=d):
-                with scope("xk%d" % k):
-                    x_relay(d, k, c)
+    def x_hop(k, quarter):
+        for part in range(PAIR):
+            for d in both:
+                @pl.when(reach(d, k)[1])
+                def _(d=d, part=part):
+                    with scope("xk%d" % k):
+                        x_relay(d, k, quarter * PAIR + part)
 
     with scope("oearly"):
         each(0, early, o_near)
@@ -659,7 +663,7 @@
         each(0, early, over)
     with scope("omid"):
         each(0, lambda at: at == 2, o_full)
-    for c in range(PARTS):
+    for c in range(PARTS // PAIR):
         x_hop(1, c)
     w_each(w_crossed, 1, lambda at: at != 2)
     for far in range(2, n):
@@ -669,13 +673,32 @@
         each(1, lambda at: at > 2, o_first)
         each(1, lambda at: at > 2, lambda d, k: o_half(d, k, 0, (Y1A, C0)))
 
-    def e_begin():
+    def e_begin(when=None):
         for o in range(1, n):
-            e_copy(o).start()
+            if when is None:
+                e_copy(o).start()
+            else:
+                pl.when(when((z + o) % n))(lambda o=o: e_copy(o).start())
+
+    at_end = lambda at: (at == 0) | (at == n - 1)
+    inside = lambda at: (at > 0) & (at < n - 1)
 
     outer = (z == 0) | (z == n - 1)
     with scope("wc"):
         local_wait(W.at[0:2], ws_recv.at[0])
+
+    param = lambda i: v_ref[i : i + 1, cols(z)]
+    shift = s_ref[z]
+    upward = 2 * z < n
+    nothing = (jnp.zeros((TILE, HEAD), jnp.float32), jnp.zeros((TILE, 1), jnp.float32))
+
+    def attend_known():
+        base = jnp.where(upward, 0, 1)
+        for a in range(n - 1):
+            carry = nothing
+            for b in range(a, -1, -1):
+                carry = attend_tile(proj, base + a, base + b, a == b, shift, carry)
+            at_total[base + a], at_keep[base + a] = carry
 
     def gather_step(k, carry):
         @pl.when(k == 1)
@@ -693,8 +716,14 @@
         def _():
             with scope("o21"):
                 each(1, lambda at: at == 2, o_full)
+            pl.when(jnp.logical_not(outer))(lambda: e_begin(inside))
 
         pl.when((k == n - 1) & outer)(e_begin)
+
+        @pl.when(k == jnp.where(outer, n - 1, n - 2))
+        def _():
+            with scope("known"):
+                attend_known()
 
         @pl.when(z - k >= 0)
         def _():
@@ -734,57 +763,92 @@
     with scope("over0"):
         each(0, lambda at: at == 2, over)
 
-    def m_copy(m, flip, o):
-        to = side if flip else x
+    def m_piece(m, block, to):
         rows = pl.ds(pl.multiple_of(to * half, half), half)
-        src = (ma, mb)[m].at[(z + o) % n, rows]
-        if o == 0 and not flip:
-            return pltpu.make_async_copy(src, M.at[m, x, z], m_recv.at[m])
-        return remote(src, M.at[m, x, z], m_send.at[0], m_recv.at[m], sp=(z + o) % n, tp=to)
+        return (ma, mb)[m].at[block, rows]
+
+    def m_send_to(m, block, flip=True):
+        into = M.at[m, x, z]
+        if flip:
+            remote(m_piece(m, block, side), into, m_send.at[0], m_recv.at[m], sp=block, tp=side).start()
+
+        @pl.when(block == z)
+        def _():
+            pltpu.make_async_copy(m_piece(m, block, x), into, m_recv.at[m]).start()
+
+        @pl.when(block != z)
+        def _():
+            remote(m_piece(m, block, x), into, m_send.at[0], m_recv.at[m], sp=block).start()
+
+    ends = tuple(enumerate((0, n - 1)))
+
+    def m_hand(m):
+        for e, block in ends:
+            remote(m_piece(m, block, side), R.at[m, e], m_send.at[0], r_recv.at[m], tp=side).start()
+
+    def m_pass(m):
+        local_wait(R.at[m], r_recv.at[m])
+        for e, block in ends:
+            remote(R.at[m, e], M.at[m, side, z], r_send.at[0], m_recv.at[m], sp=block).start()
 
     def t_copy(o):
         if o == 0:
             return pltpu.make_async_copy(ts.at[z], T.at[z], t_recv.at[0])
         return remote(ts.at[(z + o) % n], T.at[z], t_send.at[0], t_recv.at[0], sp=(z + o) % n)
 
-    ways = [(flip, o) for o in range(n - 1, -1, -1) for flip in both]
-
-    param = lambda i: v_refs[i][:, cols(z)]
-    shift = s_ref[z]
-    for i in range(n):
-        with scope('attn'):
-            mixed, keep = attend_tile(i, proj, shift, param(0))
-        ma[i] = mixed
-        total = jnp.log(jnp.maximum(1.0 - jnp.exp(keep), log_floor))
-        ts[i] = jnp.broadcast_to(total, (tokens, HEAD)).T[0:8, :]
-        if i == min(2, n - 1):
-            pl.when(jnp.logical_not(outer))(e_begin)
-        if i == min(2, n - 1):
-            with scope("o33"):
-                each(2, always, o_second)
-                each(1, lambda at: at > 2, o_got_x)
+
+    with scope("attn"):
+        for t in range(n):
+            i, j = jnp.where(upward, n - 1, t), jnp.where(upward, n - 1 - t, 0)
+            if t:
+                carry = tuple(jnp.where(upward, a, ref[t]) for a, ref in zip(carry, (at_total, at_keep)))
+            else:
+                carry = nothing
+            carry = attend_tile(proj, i, j, t == 0, shift, carry)
+            at_total[i], at_keep[i] = carry
+    with scope("attn2"):
+        for i in range(n):
+            ma[i] = head_norm(at_total[i], param(0)).astype(jnp.bfloat16)
+            total = jnp.log(jnp.maximum(1.0 - jnp.exp(at_keep[i]), log_floor))
+            ts[i] = jnp.broadcast_to(total, (tokens, HEAD)).T[0:8, :]
+    @pl.when(jnp.logical_not(outer))
+    def _():
+        e_begin(at_end)
+        for block in range(1, n - 1):
+            m_send_to(0, block)
+        m_hand(0)
+
+    @pl.when(outer)
+    def _():
+        for block in range(n):
+            m_send_to(0, block)
+
+    with scope("got"):
+        each(1, lambda at: at > 2, o_got_x)
     local[1].wait()
     with scope('ewait'):
         local_wait(E.at[1:n], e_recv.at[0])
     floor, offset, gain = param(2), param(3), param(1)
     per = tokens // CHUNK
 
-    def a_begin():
-        for way in ways:
-            m_copy(0, *way).start()
+    def t_begin():
         for o in range(n):
             t_copy(o).start()
 
     def tick0():
-        each(2, always, o_by_y)
         each(1, lambda at: at == 2, look)
 
+    def m_outward(m):
+        for _, block in ends:
+            m_send_to(m, block, False)
+
     def tick1():
-        pl.when(jnp.logical_not(outer))(a_begin)
-        each(2, always, o_got_y)
+        each(2, always, lambda d, k: o_pass(slot(d, k), (Y1B, X2)))
 
     def tick2():
-        each(2, always, o_got_x)
+        pass
+
+    each(2, always, o_second)
 
     def tick5():
         each(1, lambda at: at == 2, over)
@@ -792,7 +856,7 @@
     def tick6():
         each(1, lambda at: at > 2, over)
 
-    pl.when(outer)(a_begin)
+    t_begin()
     ticks = ((0, tick0), (1, tick1), (2, tick2))
 
     def recur_block(i, state):
@@ -801,6 +865,7 @@
             at = slice(j * CHUNK, (j + 1) * CHUNK)
             mixed, state = recur_chunk(proj, E.at[i, at], here, state, floor, offset, gain)
             mb[i, at, :] = mixed
+        pl.when(outer | inside(i))(lambda: m_send_to(1, i))
         for when, tick in ticks:
             @pl.when(i == when)
             def _(when=when, tick=tick):
@@ -811,9 +876,18 @@
     state = jnp.zeros((HEAD, HEAD), jnp.float32)
     with scope("rec"):
         lax.fori_loop(0, n, recur_block, state)
-    for way in ways:
-        m_copy(1, *way).start()
+
+    @pl.when(jnp.logical_not(outer))
+    def _():
+        m_hand(1)
+        m_outward(0)
+        m_pass(0)
+        m_outward(1)
+        m_pass(1)
+
     with scope("passes"):
+        each(2, always, lambda d, k: o_pass(slot(d, k), (X1A, Y2), (X1B, C2)))
+        each(2, always, lambda d, k: o_pass(slot(d, k), (Y1A, C1)))
         tick5()
         tick6()
     def order(s):
@@ -854,6 +928,18 @@
     lax.fori_loop(0, n - 1, first_half, 0)
     with scope("end3"):
         each(2, always, over)
+    with scope("mwait1"):
+        local_wait(M.at[1], m_recv.at[1])
+    lhs2 = [rows_of(1, t) for t in both]
+
+    def store(block, values):
+        at = pl.ds(pl.multiple_of(block * width, width), width)
+        out_ref[:, at] = values.astype(jnp.bfloat16)
+
+    with scope("outp2"):
+        for s in range(n - 1):
+            block = order(s)
+            store(block, acc[block] + times(lhs2, 1, block))
     with scope("drain"):
         local_wait(W.at[1:n], ws_send.at[0])
         local_wait(wp.at[1:n], w_send.at[0])
@@ -870,23 +956,18 @@
                     whole = O.at[z, f, x]
                     remote(whole, whole, oz_send.at[d, k], oz_recv.at[0, 0], sp=(z + 1) % n).wait_send()
 
-    lax.fori_loop(n - 1, n, first_half, 0)
     for o in range(n):
         local_wait(proj, o_send.at[o])
     local_wait(T, t_recv.at[0])
     local_wait(T.at[1:n], t_send.at[0])
     for k in range(n):
         T_ref[k : k + 1, :] = T[k, 0:1, :]
-    with scope("mwait1"):
-        local_wait(M.at[1], m_recv.at[1])
-    lhs2 = [rows_of(1, t) for t in both]
-
-    with scope("outp2"):
-        for s in range(n):
-            block = order(s)
-            at = pl.ds(pl.multiple_of(block * width, width), width)
-            out_ref[:, at] = (acc[block] + times(lhs2, 1, block)).astype(jnp.bfloat16)
+    with scope("owait"):
+        block = arrived(n - 1)
+    with scope("outl"):
+        store(block, times(lhs, 0, block) + times(lhs2, 1, block))
     local_wait(wp.at[0:2], m_send.at[0])
+    pl.when(jnp.logical_not(outer))(lambda: local_wait(R, r_send.at[0]))
 
 
 VMEM = pl.BlockSpec(memory_space=pltpu.VMEM)
@@ -927,7 +1008,7 @@
             pltpu.VMEM((half, depth), jnp.bfloat16),
             pltpu.VMEM((n, tokens), jnp.float32),
         ),
-        in_specs=[SMEM] + [VMEM] * 5 + [ANY] * 11,
+        in_specs=[SMEM] + [ANY] * 16,
         out_specs=(VMEM, VMEM),
         scratch_shapes=[
             bf(n, tokens, depth),
@@ -945,12 +1026,17 @@
             pltpu.VMEM((n, 8, tokens), jnp.float32),
             bf(2, 2, n, half, HEAD),
             pltpu.VMEM((n, half, depth // n), jnp.float32),
+            pltpu.VMEM((1, depth), jnp.float32),
+            pltpu.VMEM((4, columns), jnp.float32),
+            pltpu.VMEM((n, tokens, HEAD), jnp.float32),
+            pltpu.VMEM((n, tokens, 1), jnp.float32),
+            bf(2, 2, half, HEAD),
         ]
         + [DMA((2, n - 1)), DMA((n - 1, PARTS)), DMA((n - 1,)), DMA((n - 1,))]
         + [DMA((2, n - 1)), DMA((n - 1, 2)), DMA((n,)), DMA((C0, n)), DMA((n,))]
         + [DMA((1,)), DMA((n,)), DMA((n,)), DMA((1,)), DMA((1,))]
         + [DMA((1,)), DMA((1,)), DMA((1,)), DMA((2,)), DMA((1,)), DMA((1,))]
-        + [DMA((n,)), DMA((5,))],
+        + [DMA((n,)), DMA((5,)), DMA((5,)), DMA((1,)), DMA((2,))],
         compiler_params=pltpu.CompilerParams(
             collective_id=0, has_side_effects=True, vmem_limit_bytes=56 * 1024 * 1024
         ),
@@ -981,7 +1067,7 @@
     heads_fit = mesh.shape["fs"] == 4 and mesh.shape["tp"] == 2 and n > 1
 
     def on_device(*args):
-        if heads_fit and args[11].shape[0] == n and args[0].shape[1] == TILE:
+        if heads_fit and n == PARTS // PAIR and args[11].shape[0] == n and args[0].shape[1] == TILE:
             return on_device_heads(n, *args)
         return on_device_general(*args)
 

time: 96.1 us -> 94.3 us (0.981)
  Pallas kernels: 93.9 us -> 92.1 us
    pallas_call x1, Pallas kernels: 93.9 us -> 92.1 us  [on_device_heads(): pl.pallas_call(functools.partial(layer_kernel, n), out_shape=(pltpu.VMEM(...]
where the time goes in v4:
time: 94.3 us; the launch traced here: 94.2 us
  Pallas kernels  92.1 us (98%)
  local copies, waits for them, and re-layouts  1.39 us (1%)
    pallas_call x1, Pallas kernels, on_device_heads(): pl.pallas_call(functools.partial(layer_kernel, n), out_shape=(pltpu.VMEM(...  92.1 us

profile of v4, /device:TPU:0, one launch (start us, length us, event | category | flops | bytes accessed | tf_op | source)
XLA Modules:
  0.0 94.2 jit_solution(16062029291398635308)
XLA Ops:
  0.6 92.1 %shard_map.176 = (bf16[128,2048]{1,0:T(8,128)(2,1)S(1)}, f32[4,256]{1,0:T(4,128)S(1)}) custom-call(f32[4]{0:T(128)} %refs_0_.1, f32[1,2048]{1,0:T(1,128)} %bitcast.13, f32[1,512]{1,0:T(1,128)} %bitcast.14, f32[1,512]{1,0:T(1,128)} %bitcast.15, f32[1,512]{1,0:T(1,128)} %bitcast.16, f32[1,512]{1,0:T(1,128)} %bitcast.17, bf16[256,2048]{1,0:T(8,128)(2,1)} %bitcast.11, ...), custom_call_target="tpu_custom_call" | custom-call | tf_op jit(solution)/shard_map/pallas_call | solution.py:1005
  92.8 0.8 copy.21
  93.6 0.6 copy.22

commit v5 on v4

--- a/solution.py
+++ b/solution.py
@@ -968,6 +968,17 @@
         store(block, times(lhs, 0, block) + times(lhs2, 1, block))
     local_wait(wp.at[0:2], m_send.at[0])
     pl.when(jnp.logical_not(outer))(lambda: local_wait(R, r_send.at[0]))
+
+
+def store_kernel(out_ref, T_ref, out_hbm, T_hbm, sems):
+    copies = [
+        pltpu.make_async_copy(out_ref, out_hbm, sems.at[0]),
+        pltpu.make_async_copy(T_ref, T_hbm, sems.at[1]),
+    ]
+    for copy in copies:
+        copy.start()
+    for copy in copies:
+        copy.wait()
 
 
 VMEM = pl.BlockSpec(memory_space=pltpu.VMEM)
@@ -1059,7 +1070,17 @@
         output_weight_attention,
         emitted_projection_linear_scan,
     )
-    return (layer_out[None], T[None])
+    out, totals = pl.pallas_call(
+        store_kernel,
+        out_shape=(
+            jax.ShapeDtypeStruct((half, depth), jnp.bfloat16),
+            jax.ShapeDtypeStruct((n, tokens), jnp.float32),
+        ),
+        in_specs=[VMEM] * 2,
+        out_specs=(ANY, ANY),
+        scratch_shapes=[DMA((2,))],
+    )(pltpu.with_memory_space_constraint(layer_out, pltpu.VMEM), pltpu.with_memory_space_constraint(T, pltpu.VMEM))
+    return (out[None], totals[None])
 
 
 def solution(mesh):

time: 94.3 us -> 93.7 us (level)
  local copies, waits for them, and re-layouts: 1.39 us -> 0 us
    unnamed x2 -> x0, local copies, waits for them, and re-layouts: 1.39 us -> none
where the time goes in v5:
time: 93.7 us; the launch traced here: 93.6 us
  Pallas kernels  92.9 us (99%)
    pallas_call x1, Pallas kernels, on_device_heads(): pl.pallas_call(functools.partial(layer_kernel, n), out_shape=(pltpu.VMEM(...  92.1 us

profile of v5, /device:TPU:0, one launch (start us, length us, event | category | flops | bytes accessed | tf_op | source)
XLA Modules:
  0.0 93.6 jit_solution(12727329842699963604)
XLA Ops:
  0.6 92.1 %shard_map.176 = (bf16[128,2048]{1,0:T(8,128)(2,1)S(1)}, f32[4,256]{1,0:T(4,128)S(1)}) custom-call(f32[4]{0:T(128)} %refs_0_.1, f32[1,2048]{1,0:T(1,128)} %bitcast.11, f32[1,512]{1,0:T(1,128)} %bitcast.12, f32[1,512]{1,0:T(1,128)} %bitcast.13, f32[1,512]{1,0:T(1,128)} %bitcast.14, f32[1,512]{1,0:T(1,128)} %bitcast.15, bf16[256,2048]{1,0:T(8,128)(2,1)} %bitcast.9, ...), custom_call_target="tpu_custom_call" | custom-call | tf_op jit(solution)/shard_map/pallas_call | solution.py:1016
  92.8 0.8 shard_map.177

commit v6 on v5

--- a/solution.py
+++ b/solution.py
@@ -818,11 +818,6 @@
             m_send_to(0, block)
         m_hand(0)
 
-    @pl.when(outer)
-    def _():
-        for block in range(n):
-            m_send_to(0, block)
-
     with scope("got"):
         each(1, lambda at: at > 2, o_got_x)
     local[1].wait()
@@ -836,6 +831,11 @@
             t_copy(o).start()
 
     def tick0():
+        @pl.when(outer)
+        def _():
+            for block in range(n):
+                m_send_to(0, block)
+
         each(1, lambda at: at == 2, look)
 
     def m_outward(m):

time: 93.7 us -> 92.6 us (0.988)
  Pallas kernels: 92.9 us -> 91.8 us
    pallas_call x1, Pallas kernels: 92.1 us -> 91 us  [on_device_heads(): pl.pallas_call(functools.partial(layer_kernel, n), out_shape=(pltpu.VMEM(...]
where the time goes in v6:
time: 92.6 us; the launch traced here: 92.4 us
  Pallas kernels  91.8 us (99%)
    pallas_call x1, Pallas kernels, on_device_heads(): pl.pallas_call(functools.partial(layer_kernel, n), out_shape=(pltpu.VMEM(...  91 us

profile of v6, /device:TPU:0, one launch (start us, length us, event | category | flops | bytes accessed | tf_op | source)
XLA Modules:
  0.0 92.4 jit_solution(94583308836770255)
XLA Ops:
  0.6 91.0 %shard_map.176 = (bf16[128,2048]{1,0:T(8,128)(2,1)S(1)}, f32[4,256]{1,0:T(4,128)S(1)}) custom-call(f32[4]{0:T(128)} %refs_0_.1, f32[1,2048]{1,0:T(1,128)} %bitcast.11, f32[1,512]{1,0:T(1,128)} %bitcast.12, f32[1,512]{1,0:T(1,128)} %bitcast.13, f32[1,512]{1,0:T(1,128)} %bitcast.14, f32[1,512]{1,0:T(1,128)} %bitcast.15, bf16[256,2048]{1,0:T(8,128)(2,1)} %bitcast.9, ...), custom_call_target="tpu_custom_call" | custom-call | tf_op jit(solution)/shard_map/pallas_call | solution.py:1016
  91.6 0.8 shard_map.177

commit v7 on v6

--- a/solution.py
+++ b/solution.py
@@ -375,7 +375,7 @@
         into = wp.at[o] if o else W.at[z, f]
         return [
             pltpu.make_async_copy(
-                w.at[:, cols((z + o) % n)], into.at[:, i * HEAD : (i + 1) * HEAD], pack_sem.at[o]
+                w.at[:, cols((z + o) % n)], into.at[:, i * HEAD : (i + 1) * HEAD], pack_sem.at[0]
             )
             for i, w in enumerate(w_refs)
         ]
@@ -502,9 +502,7 @@
             for c in range(PARTS):
                 x_copy(d, 0, c).start()
     with scope("packs"):
-        for o in range(n):
-            into = wp.at[o] if o else W.at[z, f]
-            pltpu.make_async_copy(into, into, pack_sem.at[o]).wait()
+        pltpu.make_async_copy(W.at[z], W.at[z], pack_sem.at[0]).wait()
     for far in range(n - 1, 0, -1):
         @pl.when(z + far < n)
         def _(far=far):
@@ -1047,7 +1045,7 @@
         + [DMA((2, n - 1)), DMA((n - 1, 2)), DMA((n,)), DMA((C0, n)), DMA((n,))]
         + [DMA((1,)), DMA((n,)), DMA((n,)), DMA((1,)), DMA((1,))]
         + [DMA((1,)), DMA((1,)), DMA((1,)), DMA((2,)), DMA((1,)), DMA((1,))]
-        + [DMA((n,)), DMA((5,)), DMA((5,)), DMA((1,)), DMA((2,))],
+        + [DMA((1,)), DMA((5,)), DMA((5,)), DMA((1,)), DMA((2,))],
         compiler_params=pltpu.CompilerParams(
             collective_id=0, has_side_effects=True, vmem_limit_bytes=56 * 1024 * 1024
         ),

time: 92.6 us -> 92.4 us (level)
  no operation moved by 1% of the time
where the time goes in v7:
time: 92.4 us; the launch traced here: 92.3 us
  Pallas kernels  91.6 us (99%)
    pallas_call x1, Pallas kernels, on_device_heads(): pl.pallas_call(functools.partial(layer_kernel, n), out_shape=(pltpu.VMEM(...  90.8 us

profile of v7, /device:TPU:0, one launch (start us, length us, event | category | flops | bytes accessed | tf_op | source)
XLA Modules:
  0.0 92.3 jit_solution(18132412702080983677)
XLA Ops:
  0.6 90.8 %shard_map.176 = (bf16[128,2048]{1,0:T(8,128)(2,1)S(1)}, f32[4,256]{1,0:T(4,128)S(1)}) custom-call(f32[4]{0:T(128)} %refs_0_.1, f32[1,2048]{1,0:T(1,128)} %bitcast.11, f32[1,512]{1,0:T(1,128)} %bitcast.12, f32[1,512]{1,0:T(1,128)} %bitcast.13, f32[1,512]{1,0:T(1,128)} %bitcast.14, f32[1,512]{1,0:T(1,128)} %bitcast.15, bf16[256,2048]{1,0:T(8,128)(2,1)} %bitcast.9, ...), custom_call_target="tpu_custom_call" | custom-call | tf_op jit(solution)/shard_map/pallas_call | solution.py:1014
  91.5 0.8 shard_map.177
